TPU v7x, 32 devices: a whole 2x2x4 slice. The times are simulated.
32 devices in a mesh: sp: 8 (over z, y), tp: 4 (over x, core).
Axes of the slice: x: 2, y: 2, z: 4, core: 2. Of those that a mesh axis runs over, the one named last changes fastest.
Arguments:
- tokens: bfloat16 [2048, 2048], P(('sp', 'tp')), may hold values from -6 to 6
- pre_gain: float32 [2048], replicated, may hold values from 0.1 to 1.9
- w_query_ret: bfloat16 [2048, 768], P('sp', 'tp'), may hold values from -0.125 to 0.125
- w_key_ret: bfloat16 [2048, 768], P('sp', 'tp'), may hold values from -0.125 to 0.125
- w_value_ret: bfloat16 [2048, 768], P('sp', 'tp'), may hold values from -0.125 to 0.125
- w_query_att: bfloat16 [2048, 768], P('sp', 'tp'), may hold values from -0.5 to 0.5
- w_key_att: bfloat16 [2048, 256], P('sp', 'tp'), may hold values from -0.125 to 0.125
- w_value_att: bfloat16 [2048, 256], P('sp', 'tp'), may hold values from -0.125 to 0.125
- w_out_ret: bfloat16 [768, 2048], P('tp', 'sp'), may hold values from -0.15625 to 0.15625
- w_out_att: bfloat16 [768, 2048], P('tp', 'sp'), may hold values from -0.15625 to 0.15625
- retain_log: float32 [2048, 12], P('sp', 'tp')
- forget_total: float32 [12, 2048], P('tp'), as said below
Outputs:
- mixed: bfloat16 [2048, 2048], P(('sp', 'tp'))
Inputs may be any that keep to these rules, and one draw needn't show every extreme that they name: `forget_total`: never rises along positions.
All inputs are finite; a program needn't handle non-finite values.
Results may differ from a plain program's by a relative error of at most 0.019.
Values may be sent and summed in bfloat16 or wider, within the bound.
A program may use at most 64 MiB of HBM per device.

v0:
```python
import functools

import jax
import jax.numpy as jnp
import numpy as np
from jax import lax
from jax.experimental import pallas as pl
from jax.experimental.pallas import tpu as pltpu
from jax.sharding import PartitionSpec as P

HEAD = 64
EPS = 1e-06
THETA = 10000.0
F32 = jnp.float32
BF16 = jnp.bfloat16
MESH = pl.DeviceIdType.MESH
SPAN = 256
KEY_SPAN = 256
LANES = 128
CHUNKS = (4, 4, 4, 2)
HIGH = lax.Precision.HIGHEST


def ring_to_sp(place, n):
    if n % 2:
        return place
    back = place // (n // 2)
    return (1 - back) * 2 * place + back * (2 * (n - 1 - place) + 1)


def sp_to_ring(index, n):
    if n % 2:
        return index
    odd, pair = index % 2, index // 2
    return (1 - odd) * pair + odd * (n - 1 - pair)


def dot(a, b, dims=((1,), (0,))):
    return lax.dot_general(a, b, (dims, ((), ())), preferred_element_type=F32)


def kernel(
    n,
    m,
    heads,
    chunks,
    tok_hbm,
    gain_ref,
    wq_ret_hbm,
    wk_ret_hbm,
    wv_ret_hbm,
    wq_att_hbm,
    wk_att_hbm,
    wv_att_hbm,
    wo_ret_hbm,
    wo_att_hbm,
    table_hbm,
    logs_ref,
    gate_ref,
    out_ref,
    tokens,
    table,
    xbuf,
    abuf,
    bbuf,
    obuf,
    kvbuf,
    state,
    num,
    den,
    outbuf,
    rsbuf,
    *sems,
):
    (load, x_send, x_recv, a_send, a_recv, b_send, b_recv, o_send, o_recv, k_send, k_recv, r_send,
     r_recv) = sems
    me = lax.axis_index("sp")
    mine = lax.axis_index("tp")
    place = sp_to_ring(me, n)
    right = ring_to_sp((place + 1) % n, n)
    left = ring_to_sp((place + n - 1) % n, n)
    tok = xbuf.shape[0]
    rows = tok // m
    width = heads * HEAD

    half_o = wo_ret_hbm.shape[0]
    loads = [
        pltpu.make_async_copy(source, target, load.at[k])
        for k, (source, target) in enumerate((
            (wk_att_hbm, abuf.at[me, pl.ds(0, HEAD)]),
            (wv_att_hbm, abuf.at[me, pl.ds(HEAD, HEAD)]),
            (wk_ret_hbm, abuf.at[me, pl.ds(2 * HEAD, width)]),
            (wv_ret_hbm, abuf.at[me, pl.ds(2 * HEAD + width, width)]),
            (tok_hbm, tokens),
            (wq_att_hbm, bbuf.at[me, pl.ds(0, width)]),
            (wq_ret_hbm, bbuf.at[me, pl.ds(width, width)]),
            (table_hbm.at[pl.ds(pl.multiple_of(me * tok, tok), tok)], table),
            (wo_ret_hbm, obuf.at[me, pl.ds(0, half_o)]),
            (wo_att_hbm, obuf.at[me, pl.ds(half_o, wo_att_hbm.shape[0])]),
        ))
    ]
    for copy in loads:
        copy.start()

    barrier = pltpu.get_barrier_semaphore()
    for other in (left, right):
        pl.semaphore_signal(barrier, inc=1, device_id={"sp": other}, device_id_type=MESH)
    for r in range(1, m):
        pl.semaphore_signal(barrier, inc=1, device_id={"tp": (mine + r) % m}, device_id_type=MESH)

    for copy in loads[:4]:
        copy.wait()
    pl.semaphore_wait(barrier, 2 + m - 1)

    rounds = n // 2
    full = (n - 1) // 2

    def ring_copy(buf, send, recv, pieces, step, way, chunk, arriving):
        hops = step + 1 if arriving else step
        owner = ring_to_sp((place + (n - hops if way == 0 else hops)) % n, n)
        piece = buf.shape[1] // pieces
        span = pl.ds(chunk * piece, piece)
        return pltpu.make_async_remote_copy(
            src_ref=buf.at[owner, span],
            dst_ref=buf.at[owner, span],
            send_sem=send.at[way, step, chunk],
            recv_sem=recv.at[way, step, chunk],
            device_id={"sp": right if way == 0 else left},
            device_id_type=MESH,
        )

    started = []

    def travels(pieces, step, way, chunk):
        if step < full:
            return True
        return step < rounds and (chunk < pieces // 2) == (way == 0)

    def ring_step(group, step):
        for chunk in range(group[3]):
            for way in range(2):
                if step > 0 and travels(group[3], step - 1, way, chunk):
                    ring_copy(*group, step - 1, way, chunk, True).wait_recv()
                if travels(group[3], step, way, chunk):
                    copy = ring_copy(*group, step, way, chunk, False)
                    copy.start()
                    started.append(copy)

    ring_a = (abuf, a_send, a_recv, chunks[0])
    ring_b = (bbuf, b_send, b_recv, chunks[1])
    ring_o = (obuf, o_send, o_recv, chunks[2])
    ring_k = (kvbuf, k_send, k_recv, chunks[3])

    ring_step(ring_a, 0)
    loads[4].wait()
    values = tokens[...].astype(F32)
    scale = lax.rsqrt(jnp.mean(values * values, axis=-1, keepdims=True) + EPS)
    own = pl.ds(mine * rows, rows)
    xbuf[own, :] = (values * scale * gain_ref[...]).astype(BF16)
    for r in range(1, m):
        copy = pltpu.make_async_remote_copy(
            src_ref=xbuf.at[own],
            dst_ref=xbuf.at[own],
            send_sem=x_send.at[r - 1],
            recv_sem=x_recv.at[r - 1],
            device_id={"tp": (mine + r) % m},
            device_id_type=MESH,
        )
        copy.start()
        started.append(copy)
    for copy in loads[5:]:
        copy.wait()
    lines = lax.broadcasted_iota(jnp.int32, (tok, tok), 0)
    across = lax.broadcasted_iota(jnp.int32, (tok, tok), 1)
    causal = lines >= across
    upto = jnp.where(lines <= across, 1.0, 0.0)
    logs = jnp.concatenate([logs_ref[...], jnp.zeros((8 - heads, tok), F32)], axis=0)
    turned = lax.dot_general(
        logs, upto, (((1,), (0,)), ((), ())),
        preferred_element_type=F32, precision=lax.Precision.HIGHEST,
    )
    fill = jnp.zeros((LANES - 8, tok), F32)
    within = jnp.concatenate([turned, fill], axis=0).T
    gates_own = gate_ref[:, pl.ds(pl.multiple_of(me * tok, tok), tok)]
    gate_col = jnp.concatenate(
        [gates_own, jnp.zeros((LANES - heads, tok), F32)], axis=0
    ).T
    cosine, sine = table[:, : HEAD // 2], table[:, HEAD // 2 :]

    for step in range(1, rounds):
        ring_step(ring_a, step)
    ring_step(ring_b, 0)
    for r in range(1, m):
        other = pl.ds(((mine + m - r) % m) * rows, rows)
        pltpu.make_async_remote_copy(
            src_ref=xbuf.at[other],
            dst_ref=xbuf.at[other],
            send_sem=x_send.at[r - 1],
            recv_sem=x_recv.at[r - 1],
            device_id={"tp": (mine + r) % m},
            device_id_type=MESH,
        ).wait_recv()
    ring_step(ring_a, rounds)
    ring_step(ring_b, 1)

    def rope(field):
        half = HEAD // 2
        first, second = field[:, :half], field[:, half:]
        return jnp.concatenate(
            [first * cosine - second * sine, first * sine + second * cosine], axis=-1
        )

    def project(buf):
        deep = buf.shape[2]
        return sum(
            dot(xbuf[:, k * deep : (k + 1) * deep], buf[k], ((1,), (1,))) for k in range(n)
        )

    proj = project(abuf)
    pair = proj[:, : 2 * HEAD].astype(BF16)
    keys, vals, updates, marks = [], [], [], []
    for h in range(heads):
        base = 2 * HEAD + h * HEAD
        key = rope(proj[:, base : base + HEAD]).astype(BF16)
        val = proj[:, base + width : base + width + HEAD].astype(BF16)
        column = within[:, h : h + 1]
        last = column[tok - 1 :, :]
        faded = (key.astype(F32) * jnp.exp(last - column)).astype(BF16)
        updates.append(dot(faded, val, ((0,), (0,))))
        high = last.astype(BF16).astype(F32)
        low = last - high
        marks.append(jnp.broadcast_to(high, (8, HEAD)))
        marks.append(jnp.broadcast_to(low, (8, HEAD)))
        keys.append(key)
        vals.append(val)
    kvbuf[me, :tok, :] = pair
    marks.append(jnp.zeros((HEAD - 16 * heads, HEAD), F32))
    blocks = updates + [jnp.concatenate(marks, axis=0)]
    if len(blocks) % 2:
        blocks.append(jnp.zeros((HEAD, HEAD), F32))
    for k in range(0, len(blocks), 2):
        both = jnp.concatenate(blocks[k : k + 2], axis=1).astype(BF16)
        kvbuf[me, tok + k // 2 * HEAD : tok + (k // 2 + 1) * HEAD, :] = both

    def piece_of(index, k):
        lanes = slice(k % 2 * HEAD, (k % 2 + 1) * HEAD)
        return kvbuf[index, tok + k // 2 * HEAD : tok + (k // 2 + 1) * HEAD, lanes].astype(F32)

    for step in range(rounds - 1):
        ring_step(ring_k, step)
        ring_step(ring_b, step + 2)
    ring_step(ring_k, rounds - 1)
    ring_step(ring_o, 0)

    projq = project(bbuf)
    ring_step(ring_k, rounds)
    ring_step(ring_o, 1)
    local, lifts = [], []
    for h in range(heads):
        base = width + h * HEAD
        query = (rope(projq[:, base : base + HEAD]) * HEAD ** (-0.5)).astype(BF16)
        column = within[:, h : h + 1]
        gap = jnp.where(causal, column - turned[h : h + 1, :], 0.0)
        scores = dot(query, keys[h], ((1,), (1,)))
        weights = jnp.where(causal, scores * jnp.exp(gap), 0.0).astype(BF16)
        local.append(dot(weights, vals[h]))
        lifts.append((query.astype(F32) * jnp.exp(column)).astype(BF16))

    queries = [
        (projq[:, h * HEAD : (h + 1) * HEAD] * HEAD ** (-0.5)).astype(BF16) for h in range(heads)
    ]

    def attend(index, masked):
        block = kvbuf[index, :tok, :]
        key, val = block[:, :HEAD], block[:, HEAD:]
        gates = gate_ref[:, pl.ds(pl.multiple_of(index * tok, tok), tok)]
        for h in range(heads):
            logits = dot(queries[h], key, ((1,), (1,)))
            logits = logits + gate_col[:, h : h + 1] - gates[h : h + 1, :]
            if masked:
                logits = jnp.where(causal, logits, -jnp.inf)
            weights = jnp.exp(logits)
            den[h] += jnp.broadcast_to(jnp.sum(weights, axis=-1, keepdims=True), (tok, HEAD))
            num[h] += dot(weights.astype(BF16), val)

    den[...] = jnp.zeros_like(den)
    num[...] = jnp.zeros_like(num)
    state[...] = jnp.zeros_like(state)
    attend(me, True)
    pending = list(range(2, rounds + 1))
    ring_step(ring_o, pending.pop(0))
    for j in range(n - 1):
        def earlier(j=j):
            marked = piece_of(j, heads)
            for h in range(heads):
                total = marked[16 * h : 16 * h + 1] + marked[16 * h + 8 : 16 * h + 9]
                state[h] = jnp.exp(total) * state[h] + piece_of(j, h)
            attend(j, False)

        pl.when(me > j)(earlier)
        if j % 3 == 2 and len(pending) > 1:
            ring_step(ring_o, pending.pop(0))
    for step in pending:
        ring_step(ring_o, step)

    retained, attended = [], []
    for h in range(heads):
        raw = local[h] + dot(lifts[h], state[h].astype(BF16))
        centre = jnp.mean(raw, axis=-1, keepdims=True)
        spread = jnp.mean(jnp.square(raw - centre), axis=-1, keepdims=True)
        retained.append(((raw - centre) * lax.rsqrt(spread + EPS)).astype(BF16))
        attended.append((num[h] / den[h]).astype(BF16))
    mixed = jnp.concatenate(retained + attended, axis=-1)

    def out_copy(r, part, span):
        return pltpu.make_async_remote_copy(
            src_ref=outbuf.at[(mine + r) % m, :, span],
            dst_ref=rsbuf.at[mine, :, span],
            send_sem=r_send.at[r - 1, part],
            recv_sem=r_recv.at[r - 1, part],
            device_id={"tp": (mine + r) % m},
            device_id_type=MESH,
        )

    columns = obuf.shape[2]
    group = 2 if n % 2 == 0 else 1
    for part in range(n // group):
        for k in range(part * group, part * group + group):
            share = dot(mixed, obuf[k]).astype(BF16)
            outbuf[:, :, k * columns : (k + 1) * columns] = share.reshape(m, rows, columns)
        span = pl.ds(part * group * columns, group * columns)
        for r in range(1, m):
            copy = out_copy(r, part, span)
            copy.start()
            started.append(copy)
    for part in range(n // group):
        span = pl.ds(part * group * columns, group * columns)
        total = outbuf[mine, :, span].astype(F32)
        for r in range(1, m):
            other = (mine + m - r) % m
            pltpu.make_async_remote_copy(
                src_ref=rsbuf.at[other, :, span],
                dst_ref=rsbuf.at[other, :, span],
                send_sem=r_send.at[r - 1, part],
                recv_sem=r_recv.at[r - 1, part],
                device_id={"tp": (mine + r) % m},
                device_id_type=MESH,
            ).wait_recv()
            total = total + rsbuf[other, :, span].astype(F32)
        out_ref[:, span] = total.astype(BF16)

    for copy in started:
        copy.wait_send()


def body(
    n,
    m,
    tokens,
    pre_gain,
    w_query_ret,
    w_key_ret,
    w_value_ret,
    w_query_att,
    w_key_att,
    w_value_att,
    w_out_ret,
    w_out_att,
    retain_log,
    forget_total,
):
    rows, depth = tokens.shape
    tok = rows * m
    heads = retain_log.shape[1]
    half = HEAD // 2
    inverse = np.float32(THETA) ** (-np.arange(half, dtype=np.float32) / np.float32(half))
    angles = np.arange(n * tok, dtype=np.float32)[:, None] * inverse[None, :]
    table = np.concatenate([np.cos(angles), np.sin(angles)], axis=1).astype(np.float32)
    chunks = CHUNKS
    wide_a = 2 * HEAD + 2 * heads * HEAD
    wide_b = 2 * heads * HEAD
    deep = w_key_ret.shape[0]
    deep_o = w_out_ret.shape[0] + w_out_att.shape[0]
    tall = tok + (heads // 2 + 1) * HEAD
    hbm = pl.BlockSpec(memory_space=pl.ANY)
    vmem = pl.BlockSpec(memory_space=pltpu.VMEM)
    dma = pltpu.SemaphoreType.DMA
    rings = [dma((2, n // 2, c)) for c in chunks for _ in range(2)]
    parts = n // 2 if n % 2 == 0 else n
    return pl.pallas_call(
        functools.partial(kernel, n, m, heads, chunks),
        out_shape=jax.ShapeDtypeStruct((rows, depth), BF16),
        in_specs=[hbm, vmem] + [hbm] * 9 + [vmem] * 2,
        out_specs=vmem,
        scratch_shapes=[
            pltpu.VMEM(tokens.shape, BF16),
            pltpu.VMEM((tok, HEAD), F32),
            pltpu.VMEM((tok, depth), BF16),
            pltpu.VMEM((n, wide_a, deep), BF16),
            pltpu.VMEM((n, wide_b, deep), BF16),
            pltpu.VMEM((n, deep_o, w_out_ret.shape[1]), BF16),
            pltpu.VMEM((n, tall, 2 * HEAD), BF16),
            pltpu.VMEM((heads, HEAD, HEAD), F32),
            pltpu.VMEM((heads, tok, HEAD), F32),
            pltpu.VMEM((heads, tok, HEAD), F32),
            pltpu.VMEM((m, rows, depth), BF16),
            pltpu.VMEM((m, rows, depth), BF16),
            dma((10,)),
            dma((m - 1,)),
            dma((m - 1,)),
            *rings,
            dma((m - 1, parts)),
            dma((m - 1, parts)),
        ],
        compiler_params=pltpu.CompilerParams(
            collective_id=0, has_side_effects=True, vmem_limit_bytes=60 * 1024 * 1024
        ),
    )(
        tokens,
        pre_gain[None, :],
        w_query_ret.T,
        w_key_ret.T,
        w_value_ret.T,
        w_query_att.T,
        w_key_att.T,
        w_value_att.T,
        w_out_ret,
        w_out_att,
        jnp.asarray(table),
        retain_log.T,
        forget_total,
    )


def rotate(field, positions):
    half = field.shape[-1] // 2
    inverse = THETA ** (-jnp.arange(half, dtype=jnp.float32) / half)
    angles = positions[:, None] * inverse[None, :]
    cosine = jnp.cos(angles)[:, None, :]
    sine = jnp.sin(angles)[:, None, :]
    first_half = field[..., :half]
    second_half = field[..., half:]
    return jnp.concatenate(
        [first_half * cosine - second_half * sine, first_half * sine + second_half * cosine],
        axis=-1,
    )


def head_norm(values):
    centre = jnp.mean(values, axis=-1, keepdims=True)
    spread = jnp.mean(jnp.square(values - centre), axis=-1, keepdims=True)
    return (values - centre) * lax.rsqrt(spread + EPS)


def advance(state, pair):
    decay, update = pair
    return (jnp.exp(decay)[:, None, None] * state + update, state)


def plain_body(
    tokens,
    pre_gain,
    w_query_ret,
    w_key_ret,
    w_value_ret,
    w_query_att,
    w_key_att,
    w_value_att,
    w_out_ret,
    w_out_att,
    retain_log,
    forget_total,
):
    rows = tokens.astype(jnp.float32)
    normed = (
        rows * lax.rsqrt(jnp.mean(rows * rows, axis=-1, keepdims=True) + EPS) * pre_gain
    ).astype(jnp.bfloat16)
    gathered = lax.all_gather(normed, "tp", axis=0, tiled=True)
    tok_dev = gathered.shape[0]
    offset = lax.axis_index("sp") * tok_dev
    query_places = offset + jnp.arange(tok_dev, dtype=jnp.int32)
    positions = query_places.astype(jnp.float32)

    def blocked(values):
        return values.reshape((tok_dev // SPAN, SPAN) + values.shape[1:])

    pieces = (
        lax.all_gather(w_query_ret, "sp", axis=0, tiled=True),
        lax.all_gather(w_key_ret, "sp", axis=0, tiled=True),
        lax.all_gather(w_value_ret, "sp", axis=0, tiled=True),
        lax.all_gather(w_query_att, "sp", axis=0, tiled=True),
        lax.all_gather(w_key_att, "sp", axis=0, tiled=True),
        lax.all_gather(w_value_att, "sp", axis=0, tiled=True),
    )
    projected = tuple(
        (jnp.dot(gathered, piece, preferred_element_type=jnp.float32) for piece in pieces)
    )
    heads = retain_log.shape[1]
    shape = (tok_dev, heads, HEAD)
    query = blocked(
        (rotate(projected[0].reshape(shape), positions) * HEAD ** (-0.5)).astype(jnp.bfloat16)
    )
    key_rows = blocked(rotate(projected[1].reshape(shape), positions).astype(jnp.bfloat16))
    value_rows = blocked(projected[2].astype(jnp.bfloat16).reshape(shape))
    within = jnp.cumsum(blocked(retain_log), axis=1)
    causal = jnp.arange(SPAN)[:, None] >= jnp.arange(SPAN)[None, :]
    scores = jnp.einsum("bthd,bshd->bhts", query, key_rows, preferred_element_type=jnp.float32)
    turned = jnp.transpose(within, (0, 2, 1))
    gap = jnp.where(causal, turned[:, :, :, None] - turned[:, :, None, :], 0.0)
    weights = jnp.where(causal, scores * jnp.exp(gap), 0.0).astype(jnp.bfloat16)
    local = jnp.einsum("bhts,bshd->bthd", weights, value_rows, preferred_element_type=jnp.float32)
    last = within[:, -1]
    faded = (key_rows.astype(jnp.float32) * jnp.exp(last[:, None, :] - within)[..., None]).astype(
        jnp.bfloat16
    )
    updates = jnp.einsum("bshd,bshe->bhde", faded, value_rows, preferred_element_type=jnp.float32)
    zero_state = jnp.zeros((heads, HEAD, HEAD), jnp.float32)
    final, _ = lax.scan(advance, zero_state, (last, updates))
    decay_total = jnp.sum(last, axis=0)
    own_state = final.reshape(heads, HEAD * HEAD)
    every_total = lax.all_gather(
        decay_total[None].astype(jnp.bfloat16), "sp", axis=0, tiled=True
    ).astype(jnp.float32)
    every_state = lax.all_gather(
        own_state[None].astype(jnp.bfloat16), "sp", axis=0, tiled=True
    ).astype(jnp.float32)
    device_order = jnp.arange(every_total.shape[0], dtype=jnp.int32)[:, None]
    earlier = device_order < lax.axis_index("sp")
    before = jnp.sum(jnp.where(earlier, every_total, 0.0), axis=0)
    through = jnp.cumsum(every_total, axis=0)
    fading = jnp.where(earlier, jnp.exp(jnp.where(earlier, before[None, :] - through, 0.0)), 0.0)
    incoming = jnp.einsum("jh,jhe->he", fading, every_state, precision=HIGH)
    _, befores = lax.scan(advance, incoming.reshape(heads, HEAD, HEAD), (last, updates))
    lifted = (query.astype(jnp.float32) * jnp.exp(within)[..., None]).astype(jnp.bfloat16)
    carried = jnp.einsum(
        "bthd,bhde->bthe", lifted, befores.astype(jnp.bfloat16), preferred_element_type=jnp.float32
    )
    retained = (
        head_norm((local + carried).reshape(shape))
        .astype(jnp.bfloat16)
        .reshape(tok_dev, heads * HEAD)
    )
    raw_key = projected[4]
    gate_heads = forget_total.shape[0]
    kv_local = raw_key.shape[1] // HEAD
    group = gate_heads // kv_local
    query = (
        (projected[3] * HEAD ** (-0.5)).astype(jnp.bfloat16).reshape(tok_dev, kv_local, group, HEAD)
    )
    key_rows = raw_key.astype(jnp.bfloat16)
    value_rows = projected[5].astype(jnp.bfloat16)
    gate_rows = lax.dynamic_slice_in_dim(forget_total, offset, tok_dev, 1).reshape(
        kv_local, group, tok_dev
    )
    last_row = offset + tok_dev - 1
    init = (
        jnp.zeros((kv_local, group, tok_dev, HEAD), jnp.float32),
        jnp.zeros((kv_local, group, tok_dev), jnp.float32),
    )
    key_piece = lax.all_gather(key_rows, "sp", axis=0, tiled=True)
    value_piece = lax.all_gather(value_rows, "sp", axis=0, tiled=True)
    count = key_piece.shape[0] // KEY_SPAN

    def one_block(index, inner):
        first = index * KEY_SPAN

        def compute(state):
            weighted, total = state
            key_block = lax.dynamic_slice_in_dim(key_piece, index * KEY_SPAN, KEY_SPAN, 0).reshape(
                KEY_SPAN, kv_local, HEAD
            )
            value_block = lax.dynamic_slice_in_dim(
                value_piece, index * KEY_SPAN, KEY_SPAN, 0
            ).reshape(KEY_SPAN, kv_local, HEAD)
            gate_keys = lax.dynamic_slice_in_dim(forget_total, first, KEY_SPAN, 1).reshape(
                kv_local, group, KEY_SPAN
            )
            scores = jnp.einsum(
                "tcgd,scd->cgts", query, key_block, preferred_element_type=jnp.float32
            )
            logits = scores + gate_rows[:, :, :, None] - gate_keys[:, :, None, :]
            allowed = (first + jnp.arange(KEY_SPAN, dtype=jnp.int32))[None, :] <= query_places[
                :, None
            ]
            weights = jnp.exp(jnp.where(allowed, logits, -jnp.inf))
            total = total + jnp.sum(weights, axis=-1)
            weighted = weighted + jnp.einsum(
                "cgts,scd->cgtd",
                weights.astype(jnp.bfloat16),
                value_block,
                preferred_element_type=jnp.float32,
            )
            return (weighted, total)

        def skipped(state):
            return state

        return lax.cond(first <= last_row, compute, skipped, inner)

    weighted, total = lax.fori_loop(0, count, one_block, init)
    result = weighted / total[..., None]
    attended = (
        jnp.transpose(result, (2, 0, 1, 3)).reshape(tok_dev, gate_heads * HEAD).astype(jnp.bfloat16)
    )
    out_ret, out_att = (
        lax.all_gather(w_out_ret, "sp", axis=1, tiled=True),
        lax.all_gather(w_out_att, "sp", axis=1, tiled=True),
    )
    return lax.psum_scatter(
        (
            jnp.dot(retained, out_ret, preferred_element_type=jnp.float32)
            + jnp.dot(attended, out_att, preferred_element_type=jnp.float32)
        ).astype(jnp.bfloat16),
        "tp",
        scatter_dimension=0,
        tiled=True,
    )


def choose(n, m, *arrays):
    tokens, w_key_ret, w_out_ret = arrays[0], arrays[3], arrays[8]
    whole_tiles = w_out_ret.shape[1] % LANES == 0 and w_key_ret.shape[0] % LANES == 0
    heads = arrays[10].shape[1]
    small = 16 * heads <= HEAD and arrays[7].shape[1] == HEAD and arrays[11].shape[0] == heads
    if n % 2 == 0 and n > 2 and whole_tiles and small and tokens.shape[0] * m == SPAN:
        return body(n, m, *arrays)
    return plain_body(*arrays)


def solution(mesh):
    return jax.shard_map(
        functools.partial(choose, mesh.shape["sp"], mesh.shape["tp"]),
        mesh=mesh,
        in_specs=(
            P(("sp", "tp"), None),
            P(),
            P("sp", "tp"),
            P("sp", "tp"),
            P("sp", "tp"),
            P("sp", "tp"),
            P("sp", "tp"),
            P("sp", "tp"),
            P("tp", "sp"),
            P("tp", "sp"),
            P("sp", "tp"),
            P("tp", None),
        ),
        out_specs=P(("sp", "tp"), None),
        check_vma=False,
    )
```

profile of v0, /device:TPU:0, one launch (start us, length us, event | category | flops | bytes accessed | tf_op | source)
XLA Modules:
  0.0 82.5 jit_solution(15576057462316063861)
XLA Ops:
  0.0 80.9 %shard_map.127 = bf16[64,2048]{1,0:T(8,128)(2,1)} custom-call(bf16[64,2048]{1,0:T(8,128)(2,1)} %tok_hbm.1, f32[1,2048]{1,0:T(1,128)} %bitcast.14, bf16[192,256]{1,0:T(8,128)(2,1)} %bitcast.8, bf16[192,256]{1,0:T(8,128)(2,1)} %bitcast.9, bf16[192,256]{1,0:T(8,128)(2,1)} %bitcast.10, bf16[192,256]{1,0:T(8,128)(2,1)} %bitcast.11, bf16[64,256]{1,0:T(8,128)(2,1)} %bitcast.12, ...), custom_call_target="tpu_custom_call" | custom-call | tf_op jit(solution)/shard_map/pallas_call | solution.py:390
  80.9 1.7 %copy.15 = bf16[64,2048]{1,0:T(8,128)(2,1)} copy(bf16[64,2048]{1,0:T(8,128)(2,1)} %shard_map.127) | data formatting | bytes 524288
where the time goes:
time: 82.8 us; the launch traced here: 82.5 us
  Pallas kernels  80.9 us (98%)
  local copies, waits for them, and re-layouts  1.67 us (2%)
    pallas_call x1, Pallas kernels, body(): pl.pallas_call(functools.partial(kernel, n, m, heads, chunks), out_shape=...  80.9 us
    unnamed x1, local copies, waits for them, and re-layouts  1.67 us

commit v1 on v0

--- a/solution.py
+++ b/solution.py
@@ -17,22 +17,7 @@
 SPAN = 256
 KEY_SPAN = 256
 LANES = 128
-CHUNKS = (4, 4, 4, 2)
 HIGH = lax.Precision.HIGHEST
-
-
-def ring_to_sp(place, n):
-    if n % 2:
-        return place
-    back = place // (n // 2)
-    return (1 - back) * 2 * place + back * (2 * (n - 1 - place) + 1)
-
-
-def sp_to_ring(index, n):
-    if n % 2:
-        return index
-    odd, pair = index % 2, index // 2
-    return (1 - odd) * pair + odd * (n - 1 - pair)
 
 
 def dot(a, b, dims=((1,), (0,))):
@@ -43,7 +28,6 @@
     n,
     m,
     heads,
-    chunks,
     tok_hbm,
     gain_ref,
     wq_ret_hbm,
@@ -55,11 +39,13 @@
     wo_ret_hbm,
     wo_att_hbm,
     table_hbm,
-    logs_ref,
-    gate_ref,
+    logs_hbm,
+    gate_hbm,
     out_ref,
     tokens,
     table,
+    lbuf,
+    gbuf,
     xbuf,
     abuf,
     bbuf,
@@ -70,142 +56,235 @@
     den,
     outbuf,
     rsbuf,
-    *sems,
+    load,
+    small_send,
+    small_recv,
+    x_send,
+    x_fwd,
+    x_recv,
+    w_send,
+    w_part,
+    w_y,
+    w_recv,
+    k_send,
+    k_y,
+    k_part,
+    k_recv,
+    r_send,
+    r_recv,
 ):
-    (load, x_send, x_recv, a_send, a_recv, b_send, b_recv, o_send, o_recv, k_send, k_recv, r_send,
-     r_recv) = sems
-    me = lax.axis_index("sp")
-    mine = lax.axis_index("tp")
-    place = sp_to_ring(me, n)
-    right = ring_to_sp((place + 1) % n, n)
-    left = ring_to_sp((place + n - 1) % n, n)
-    tok = xbuf.shape[0]
-    rows = tok // m
+    s, t = lax.axis_index("sp"), lax.axis_index("tp")
+    nh, nx = n // 4, m // 2
+    y, zl, zh = s % 2, (s // 2) % 2, s // 4
+    c, x = t % 2, t // 2
+    own = zl == c
+    apart = zl != c
+
+    def sp_of(zh_, zl_, y_):
+        return zh_ * 4 + zl_ * 2 + y_
+
+    def tp_of(x_, c_):
+        return x_ * 2 + c_
+
+    def device(zh_, zl_, y_, x_, c_):
+        return {"sp": sp_of(zh_, zl_, y_), "tp": tp_of(x_, c_)}
+
+    q, g = sp_of(zh, c, y), tp_of(x, zl)
+    partner = device(zh, zl, y, x, 1 - c)
+    across = device(zh, zl, 1 - y, x, c)
+    rows = tokens.shape[0]
+    tok = rows * m
     width = heads * HEAD
-
     half_o = wo_ret_hbm.shape[0]
+
+    slot = jnp.where(own, s, n)
+    piece = jnp.where(own, t, m)
     loads = [
         pltpu.make_async_copy(source, target, load.at[k])
         for k, (source, target) in enumerate((
-            (wk_att_hbm, abuf.at[me, pl.ds(0, HEAD)]),
-            (wv_att_hbm, abuf.at[me, pl.ds(HEAD, HEAD)]),
-            (wk_ret_hbm, abuf.at[me, pl.ds(2 * HEAD, width)]),
-            (wv_ret_hbm, abuf.at[me, pl.ds(2 * HEAD + width, width)]),
             (tok_hbm, tokens),
-            (wq_att_hbm, bbuf.at[me, pl.ds(0, width)]),
-            (wq_ret_hbm, bbuf.at[me, pl.ds(width, width)]),
-            (table_hbm.at[pl.ds(pl.multiple_of(me * tok, tok), tok)], table),
-            (wo_ret_hbm, obuf.at[me, pl.ds(0, half_o)]),
-            (wo_att_hbm, obuf.at[me, pl.ds(half_o, wo_att_hbm.shape[0])]),
+            (wk_att_hbm, abuf.at[slot, pl.ds(0, HEAD)]),
+            (wv_att_hbm, abuf.at[slot, pl.ds(HEAD, HEAD)]),
+            (wk_ret_hbm, abuf.at[slot, pl.ds(2 * HEAD, width)]),
+            (wv_ret_hbm, abuf.at[slot, pl.ds(2 * HEAD + width, width)]),
+            (wq_att_hbm, bbuf.at[slot, pl.ds(0, width)]),
+            (wq_ret_hbm, bbuf.at[slot, pl.ds(width, width)]),
+            (wo_ret_hbm, obuf.at[slot, pl.ds(0, half_o)]),
+            (wo_att_hbm, obuf.at[slot, pl.ds(half_o, wo_att_hbm.shape[0])]),
+            (table_hbm.at[pl.ds(pl.multiple_of(q * tok, tok), tok)], table),
+            (logs_hbm, lbuf.at[0]),
+            (gate_hbm, gbuf.at[0]),
         ))
     ]
     for copy in loads:
         copy.start()
 
     barrier = pltpu.get_barrier_semaphore()
-    for other in (left, right):
-        pl.semaphore_signal(barrier, inc=1, device_id={"sp": other}, device_id_type=MESH)
-    for r in range(1, m):
-        pl.semaphore_signal(barrier, inc=1, device_id={"tp": (mine + r) % m}, device_id_type=MESH)
-
-    for copy in loads[:4]:
-        copy.wait()
-    pl.semaphore_wait(barrier, 2 + m - 1)
-
-    rounds = n // 2
-    full = (n - 1) // 2
-
-    def ring_copy(buf, send, recv, pieces, step, way, chunk, arriving):
-        hops = step + 1 if arriving else step
-        owner = ring_to_sp((place + (n - hops if way == 0 else hops)) % n, n)
-        piece = buf.shape[1] // pieces
-        span = pl.ds(chunk * piece, piece)
-        return pltpu.make_async_remote_copy(
-            src_ref=buf.at[owner, span],
-            dst_ref=buf.at[owner, span],
-            send_sem=send.at[way, step, chunk],
-            recv_sem=recv.at[way, step, chunk],
-            device_id={"sp": right if way == 0 else left},
-            device_id_type=MESH,
+    greeted = [across]
+    for i in reversed(range(nh)):
+        for j in reversed(range(2)):
+            for k in range(2):
+                if i or j or k:
+                    greeted.append(device((zh + i) % nh, (zl + j) % 2, y, x, (c + k) % 2))
+    for r in range(1, nx):
+        for j in range(2):
+            for k in range(2):
+                greeted.append(device(zh, (zl + j) % 2, y, (x + r) % nx, (c + k) % 2))
+    for other in greeted:
+        pl.semaphore_signal(barrier, inc=1, device_id=other, device_id_type=MESH)
+
+    started = []
+
+    def guarded(condition, action):
+        if condition is None:
+            action()
+        else:
+            pl.when(condition)(action)
+
+    def send(source, target, send_sem, recv_sem, where, condition=None):
+        copy = pltpu.make_async_remote_copy(
+            src_ref=source, dst_ref=target, send_sem=send_sem, recv_sem=recv_sem,
+            device_id=where, device_id_type=MESH,
         )
-
-    started = []
-
-    def travels(pieces, step, way, chunk):
-        if step < full:
-            return True
-        return step < rounds and (chunk < pieces // 2) == (way == 0)
-
-    def ring_step(group, step):
-        for chunk in range(group[3]):
-            for way in range(2):
-                if step > 0 and travels(group[3], step - 1, way, chunk):
-                    ring_copy(*group, step - 1, way, chunk, True).wait_recv()
-                if travels(group[3], step, way, chunk):
-                    copy = ring_copy(*group, step, way, chunk, False)
-                    copy.start()
-                    started.append(copy)
-
-    ring_a = (abuf, a_send, a_recv, chunks[0])
-    ring_b = (bbuf, b_send, b_recv, chunks[1])
-    ring_o = (obuf, o_send, o_recv, chunks[2])
-    ring_k = (kvbuf, k_send, k_recv, chunks[3])
-
-    ring_step(ring_a, 0)
-    loads[4].wait()
+        guarded(condition, copy.start)
+        started.append((copy, condition))
+
+    def receive(target, recv_sem, condition=None):
+        copy = pltpu.make_async_remote_copy(
+            src_ref=target, dst_ref=target, send_sem=recv_sem, recv_sem=recv_sem,
+            device_id=partner, device_id_type=MESH,
+        )
+        guarded(condition, copy.wait_recv)
+
+    loads[0].wait()
     values = tokens[...].astype(F32)
     scale = lax.rsqrt(jnp.mean(values * values, axis=-1, keepdims=True) + EPS)
-    own = pl.ds(mine * rows, rows)
-    xbuf[own, :] = (values * scale * gain_ref[...]).astype(BF16)
-    for r in range(1, m):
-        copy = pltpu.make_async_remote_copy(
-            src_ref=xbuf.at[own],
-            dst_ref=xbuf.at[own],
-            send_sem=x_send.at[r - 1],
-            recv_sem=x_recv.at[r - 1],
-            device_id={"tp": (mine + r) % m},
-            device_id_type=MESH,
+    xbuf[pl.ds(pl.multiple_of(piece * rows, rows), rows), :] = (
+        values * scale * gain_ref[...]
+    ).astype(BF16)
+    for copy in loads[1:]:
+        copy.wait()
+    pl.semaphore_wait(barrier, len(greeted))
+
+    parts = (abuf, bbuf, obuf)
+
+    def half(buf, index, k):
+        length = buf.shape[1] // 2
+        return buf.at[index, pl.ds(pl.multiple_of(k * length, length), length)]
+
+    def scatter(p, i):
+        buf = parts[p]
+        for k in (1, 0):
+            core = (c + k) % 2
+            send(
+                half(buf, slot, core), half(buf, s, core),
+                w_send.at[p, i, k], w_recv.at[p, s, core],
+                device((zh + i) % nh, c, y, x, core),
+                apart if i == 0 and k == 0 else None,
+            )
+
+    def entry(p, i, j):
+        buf = parts[p]
+        index = sp_of((zh + i) % nh, (zl + j) % 2, y)
+        here = i == 0 and j == 0
+        spot = half(buf, index, c)
+        receive(spot, w_recv.at[p, index, c], apart if here else None)
+        send(spot, spot, w_y.at[p, i, j], w_recv.at[p, index, c], across)
+        send(
+            spot, spot, w_part.at[p, i, j, 0], w_recv.at[p, index, c], partner,
+            own if here else None,
         )
-        copy.start()
-        started.append(copy)
-    for copy in loads[5:]:
-        copy.wait()
+
+    def beside(p, i, j):
+        buf = parts[p]
+        index = sp_of((zh + i) % nh, (zl + j) % 2, 1 - y)
+        spot = half(buf, index, c)
+        receive(spot, w_recv.at[p, index, c])
+        send(spot, spot, w_part.at[p, i, j, 1], w_recv.at[p, index, c], partner)
+
+    def rest(p):
+        buf = parts[p]
+        for i in range(nh):
+            for j in range(2):
+                for k in range(2):
+                    index = sp_of((zh + i) % nh, (zl + j) % 2, (y + k) % 2)
+                    receive(
+                        half(buf, index, 1 - c), w_recv.at[p, index, 1 - c],
+                        apart if i == 0 and j == 0 and k == 0 else None,
+                    )
+
+    order = [(i, j) for i in range(nh) for j in range(2)]
+
+    def rows_of(index):
+        return xbuf.at[pl.ds(pl.multiple_of(index * rows, rows), rows)]
+
+    scatter(0, 0)
+    entry_first = order[0]
+    send(rows_of(piece), rows_of(t), x_send.at[0], x_recv.at[t], device(zh, 1 - zl, y, x, zl))
+    for r in range(1, nx):
+        send(
+            rows_of(piece), rows_of(t), x_send.at[1 + r], x_recv.at[t],
+            device(zh, zl, y, (x + r) % nx, zl),
+        )
+    send(rows_of(piece), rows_of(t), x_send.at[1], x_recv.at[t], device(zh, zl, y, x, zl), apart)
+    send(
+        lbuf.at[0], lbuf.at[1], small_send.at[0], small_recv.at[0],
+        device(zh, c, y, x, zl), apart,
+    )
+    send(gbuf.at[0], gbuf.at[1], small_send.at[1], small_recv.at[1], partner, own)
+    for i in range(1, nh):
+        scatter(0, i)
+    entry(0, *entry_first)
+    for i in range(nh):
+        scatter(1, i)
+
+    def pass_tokens(k):
+        index = tp_of(x, (c + k) % 2)
+        spot = rows_of(index)
+        receive(spot, x_recv.at[index], apart if k == 0 else None)
+        for r in range(1, nx):
+            send(
+                spot, spot, x_fwd.at[r - 1, k], x_recv.at[index],
+                device(zh, zl, y, (x + r) % nx, c), apart,
+            )
+
+    entry(0, *order[1])
+    beside(0, *order[0])
+    for k in range(2):
+        pass_tokens(k)
+    for a in range(2, len(order)):
+        entry(0, *order[a])
+        beside(0, *order[a - 1])
+    beside(0, *order[-1])
+
     lines = lax.broadcasted_iota(jnp.int32, (tok, tok), 0)
-    across = lax.broadcasted_iota(jnp.int32, (tok, tok), 1)
-    causal = lines >= across
-    upto = jnp.where(lines <= across, 1.0, 0.0)
-    logs = jnp.concatenate([logs_ref[...], jnp.zeros((8 - heads, tok), F32)], axis=0)
+    lanes = lax.broadcasted_iota(jnp.int32, (tok, tok), 1)
+    causal = lines >= lanes
+    upto = jnp.where(lines <= lanes, 1.0, 0.0)
+    receive(lbuf.at[1], small_recv.at[0], apart)
+    receive(gbuf.at[1], small_recv.at[1], apart)
+    pick = jnp.where(own, 0, 1)
+    logs = jnp.concatenate([lbuf[pick], jnp.zeros((8 - heads, tok), F32)], axis=0)
     turned = lax.dot_general(
         logs, upto, (((1,), (0,)), ((), ())),
         preferred_element_type=F32, precision=lax.Precision.HIGHEST,
     )
     fill = jnp.zeros((LANES - 8, tok), F32)
     within = jnp.concatenate([turned, fill], axis=0).T
-    gates_own = gate_ref[:, pl.ds(pl.multiple_of(me * tok, tok), tok)]
+    gates_own = gbuf[pick, :, pl.ds(pl.multiple_of(q * tok, tok), tok)]
     gate_col = jnp.concatenate(
         [gates_own, jnp.zeros((LANES - heads, tok), F32)], axis=0
     ).T
     cosine, sine = table[:, : HEAD // 2], table[:, HEAD // 2 :]
 
-    for step in range(1, rounds):
-        ring_step(ring_a, step)
-    ring_step(ring_b, 0)
-    for r in range(1, m):
-        other = pl.ds(((mine + m - r) % m) * rows, rows)
-        pltpu.make_async_remote_copy(
-            src_ref=xbuf.at[other],
-            dst_ref=xbuf.at[other],
-            send_sem=x_send.at[r - 1],
-            recv_sem=x_recv.at[r - 1],
-            device_id={"tp": (mine + r) % m},
-            device_id_type=MESH,
-        ).wait_recv()
-    ring_step(ring_a, rounds)
-    ring_step(ring_b, 1)
+    for r in range(1, nx):
+        for k in range(2):
+            index = tp_of((x + r) % nx, k)
+            receive(rows_of(index), x_recv.at[index])
+    rest(0)
 
     def rope(field):
-        half = HEAD // 2
-        first, second = field[:, :half], field[:, half:]
+        first, second = field[:, : HEAD // 2], field[:, HEAD // 2 :]
         return jnp.concatenate(
             [first * cosine - second * sine, first * sine + second * cosine], axis=-1
         )
@@ -213,7 +292,7 @@
     def project(buf):
         deep = buf.shape[2]
         return sum(
-            dot(xbuf[:, k * deep : (k + 1) * deep], buf[k], ((1,), (1,))) for k in range(n)
+            dot(xbuf[:tok, k * deep : (k + 1) * deep], buf[k], ((1,), (1,))) for k in range(n)
         )
 
     proj = project(abuf)
@@ -233,28 +312,56 @@
         marks.append(jnp.broadcast_to(low, (8, HEAD)))
         keys.append(key)
         vals.append(val)
-    kvbuf[me, :tok, :] = pair
+    kvbuf[q, :tok, :] = pair
     marks.append(jnp.zeros((HEAD - 16 * heads, HEAD), F32))
     blocks = updates + [jnp.concatenate(marks, axis=0)]
     if len(blocks) % 2:
         blocks.append(jnp.zeros((HEAD, HEAD), F32))
     for k in range(0, len(blocks), 2):
         both = jnp.concatenate(blocks[k : k + 2], axis=1).astype(BF16)
-        kvbuf[me, tok + k // 2 * HEAD : tok + (k // 2 + 1) * HEAD, :] = both
+        kvbuf[q, tok + k // 2 * HEAD : tok + (k // 2 + 1) * HEAD, :] = both
 
     def piece_of(index, k):
-        lanes = slice(k % 2 * HEAD, (k % 2 + 1) * HEAD)
-        return kvbuf[index, tok + k // 2 * HEAD : tok + (k // 2 + 1) * HEAD, lanes].astype(F32)
-
-    for step in range(rounds - 1):
-        ring_step(ring_k, step)
-        ring_step(ring_b, step + 2)
-    ring_step(ring_k, rounds - 1)
-    ring_step(ring_o, 0)
+        spot = slice(k % 2 * HEAD, (k % 2 + 1) * HEAD)
+        return kvbuf[index, tok + k // 2 * HEAD : tok + (k // 2 + 1) * HEAD, spot].astype(F32)
+
+    def share(index, sem, where, condition=None):
+        send(kvbuf.at[index], kvbuf.at[index], sem, k_recv.at[index], where, condition)
+
+    def arrive(index, condition=None):
+        receive(kvbuf.at[index], k_recv.at[index], condition)
+
+    for i in range(1, nh):
+        share(q, k_send.at[i - 1], device((zh + i) % nh, zl, y, x, c), zh + i < nh)
+    share(q, k_y.at[0], across, c + y < 2)
+    share(q, k_part.at[0, 0], partner, c == 0)
+    for i in range(nh):
+        scatter(2, i)
+
+    for a in range(len(order)):
+        entry(1, *order[a])
+        if a:
+            beside(1, *order[a - 1])
+        if a == 0:
+            index = sp_of(zh, c, 1 - y)
+            arrive(index, c <= y)
+            share(index, k_part.at[0, 1], partner, c == 0)
+    for i in range(1, nh):
+        index = sp_of((zh + nh - i) % nh, c, y)
+        arrive(index, zh >= i)
+        share(index, k_y.at[i], across, zh >= i)
+        share(index, k_part.at[i, 0], partner, zh >= i)
+    beside(1, *order[-1])
+    entry(2, *order[0])
+    for i in range(1, nh):
+        index = sp_of((zh + nh - i) % nh, c, 1 - y)
+        arrive(index, zh >= i)
+        share(index, k_part.at[i, 1], partner, zh >= i)
+    rest(1)
 
     projq = project(bbuf)
-    ring_step(ring_k, rounds)
-    ring_step(ring_o, 1)
+    entry(2, *order[1])
+    beside(2, *order[0])
     local, lifts = [], []
     for h in range(heads):
         base = width + h * HEAD
@@ -273,7 +380,7 @@
     def attend(index, masked):
         block = kvbuf[index, :tok, :]
         key, val = block[:, :HEAD], block[:, HEAD:]
-        gates = gate_ref[:, pl.ds(pl.multiple_of(index * tok, tok), tok)]
+        gates = gbuf[pick, :, pl.ds(pl.multiple_of(index * tok, tok), tok)]
         for h in range(heads):
             logits = dot(queries[h], key, ((1,), (1,)))
             logits = logits + gate_col[:, h : h + 1] - gates[h : h + 1, :]
@@ -286,9 +393,21 @@
     den[...] = jnp.zeros_like(den)
     num[...] = jnp.zeros_like(num)
     state[...] = jnp.zeros_like(state)
-    attend(me, True)
-    pending = list(range(2, rounds + 1))
-    ring_step(ring_o, pending.pop(0))
+    attend(q, True)
+    entry(2, *order[2])
+    beside(2, *order[1])
+    for k in range(2):
+        arrive(sp_of(zh, 1 - c, (y + k) % 2), c == 1)
+    for i in range(1, nh):
+        for k in range(2):
+            arrive(sp_of((zh + nh - i) % nh, 1 - c, (y + k) % 2), zh >= i)
+    pending = [(entry, a) for a in order[3:]]
+    after = [(beside, a) for a in order[2:]]
+    steps = []
+    for a in range(len(after)):
+        if a < len(pending):
+            steps.append(pending[a])
+        steps.append(after[a])
     for j in range(n - 1):
         def earlier(j=j):
             marked = piece_of(j, heads)
@@ -297,11 +416,13 @@
                 state[h] = jnp.exp(total) * state[h] + piece_of(j, h)
             attend(j, False)
 
-        pl.when(me > j)(earlier)
-        if j % 3 == 2 and len(pending) > 1:
-            ring_step(ring_o, pending.pop(0))
-    for step in pending:
-        ring_step(ring_o, step)
+        pl.when(q > j)(earlier)
+        if j % 2 == 0 and steps:
+            call, a = steps.pop(0)
+            call(2, *a)
+    for call, a in steps:
+        call(2, *a)
+    rest(2)
 
     retained, attended = [], []
     for h in range(heads):
@@ -312,45 +433,43 @@
         attended.append((num[h] / den[h]).astype(BF16))
     mixed = jnp.concatenate(retained + attended, axis=-1)
 
-    def out_copy(r, part, span):
-        return pltpu.make_async_remote_copy(
-            src_ref=outbuf.at[(mine + r) % m, :, span],
-            dst_ref=rsbuf.at[mine, :, span],
-            send_sem=r_send.at[r - 1, part],
-            recv_sem=r_recv.at[r - 1, part],
-            device_id={"tp": (mine + r) % m},
-            device_id_type=MESH,
-        )
-
     columns = obuf.shape[2]
-    group = 2 if n % 2 == 0 else 1
+    group = 2
     for part in range(n // group):
         for k in range(part * group, part * group + group):
-            share = dot(mixed, obuf[k]).astype(BF16)
-            outbuf[:, :, k * columns : (k + 1) * columns] = share.reshape(m, rows, columns)
+            term = dot(mixed, obuf[k]).astype(BF16)
+            outbuf[:, :, k * columns : (k + 1) * columns] = term.reshape(m, rows, columns)
         span = pl.ds(part * group * columns, group * columns)
-        for r in range(1, m):
-            copy = out_copy(r, part, span)
-            copy.start()
-            started.append(copy)
+        for r in reversed(range(nx)):
+            for k in range(2):
+                index = tp_of((x + r) % nx, (c + k) % 2)
+                send(
+                    outbuf.at[index, :, span], rsbuf.at[g, :, span],
+                    r_send.at[part, r, k], r_recv.at[part, g],
+                    device(zh, c, y, (x + r) % nx, (c + k) % 2),
+                    apart if r == 0 and k == 0 else None,
+                )
     for part in range(n // group):
         span = pl.ds(part * group * columns, group * columns)
-        total = outbuf[mine, :, span].astype(F32)
-        for r in range(1, m):
-            other = (mine + m - r) % m
-            pltpu.make_async_remote_copy(
-                src_ref=rsbuf.at[other, :, span],
-                dst_ref=rsbuf.at[other, :, span],
-                send_sem=r_send.at[r - 1, part],
-                recv_sem=r_recv.at[r - 1, part],
-                device_id={"tp": (mine + r) % m},
-                device_id_type=MESH,
-            ).wait_recv()
-            total = total + rsbuf[other, :, span].astype(F32)
+
+        def keep():
+            rsbuf[g, :, span] = outbuf[t, :, span]
+
+        pl.when(own)(keep)
+        total = None
+        for r in range(nx):
+            for j in range(2):
+                index = tp_of((x + r) % nx, (zl + j) % 2)
+                receive(
+                    rsbuf.at[index, :, span], r_recv.at[part, index],
+                    apart if r == 0 and j == 0 else None,
+                )
+                term = rsbuf[index, :, span].astype(F32)
+                total = term if total is None else total + term
         out_ref[:, span] = total.astype(BF16)
 
-    for copy in started:
-        copy.wait_send()
+    for copy, condition in started:
+        guarded(condition, copy.wait_send)
 
 
 def body(
@@ -372,11 +491,11 @@
     rows, depth = tokens.shape
     tok = rows * m
     heads = retain_log.shape[1]
+    nh, nx = n // 4, m // 2
     half = HEAD // 2
     inverse = np.float32(THETA) ** (-np.arange(half, dtype=np.float32) / np.float32(half))
     angles = np.arange(n * tok, dtype=np.float32)[:, None] * inverse[None, :]
     table = np.concatenate([np.cos(angles), np.sin(angles)], axis=1).astype(np.float32)
-    chunks = CHUNKS
     wide_a = 2 * HEAD + 2 * heads * HEAD
     wide_b = 2 * heads * HEAD
     deep = w_key_ret.shape[0]
@@ -385,32 +504,42 @@
     hbm = pl.BlockSpec(memory_space=pl.ANY)
     vmem = pl.BlockSpec(memory_space=pltpu.VMEM)
     dma = pltpu.SemaphoreType.DMA
-    rings = [dma((2, n // 2, c)) for c in chunks for _ in range(2)]
-    parts = n // 2 if n % 2 == 0 else n
     return pl.pallas_call(
-        functools.partial(kernel, n, m, heads, chunks),
+        functools.partial(kernel, n, m, heads),
         out_shape=jax.ShapeDtypeStruct((rows, depth), BF16),
-        in_specs=[hbm, vmem] + [hbm] * 9 + [vmem] * 2,
+        in_specs=[hbm, vmem] + [hbm] * 11,
         out_specs=vmem,
         scratch_shapes=[
             pltpu.VMEM(tokens.shape, BF16),
             pltpu.VMEM((tok, HEAD), F32),
-            pltpu.VMEM((tok, depth), BF16),
-            pltpu.VMEM((n, wide_a, deep), BF16),
-            pltpu.VMEM((n, wide_b, deep), BF16),
-            pltpu.VMEM((n, deep_o, w_out_ret.shape[1]), BF16),
+            pltpu.VMEM((2,) + retain_log.shape[::-1], F32),
+            pltpu.VMEM((2,) + forget_total.shape, F32),
+            pltpu.VMEM((tok + rows, depth), BF16),
+            pltpu.VMEM((n + 1, wide_a, deep), BF16),
+            pltpu.VMEM((n + 1, wide_b, deep), BF16),
+            pltpu.VMEM((n + 1, deep_o, w_out_ret.shape[1]), BF16),
             pltpu.VMEM((n, tall, 2 * HEAD), BF16),
             pltpu.VMEM((heads, HEAD, HEAD), F32),
             pltpu.VMEM((heads, tok, HEAD), F32),
             pltpu.VMEM((heads, tok, HEAD), F32),
             pltpu.VMEM((m, rows, depth), BF16),
             pltpu.VMEM((m, rows, depth), BF16),
-            dma((10,)),
-            dma((m - 1,)),
-            dma((m - 1,)),
-            *rings,
-            dma((m - 1, parts)),
-            dma((m - 1, parts)),
+            dma((12,)),
+            dma((2,)),
+            dma((2,)),
+            dma((1 + nx,)),
+            dma((nx - 1, 2)),
+            dma((m,)),
+            dma((3, nh, 2)),
+            dma((3, nh, 2, 2)),
+            dma((3, nh, 2)),
+            dma((3, n, 2)),
+            dma((nh - 1,)),
+            dma((nh,)),
+            dma((nh, 2)),
+            dma((n,)),
+            dma((n // 2, nx, 2)),
+            dma((n // 2, m)),
         ],
         compiler_params=pltpu.CompilerParams(
             collective_id=0, has_side_effects=True, vmem_limit_bytes=60 * 1024 * 1024
@@ -622,7 +751,8 @@
     whole_tiles = w_out_ret.shape[1] % LANES == 0 and w_key_ret.shape[0] % LANES == 0
     heads = arrays[10].shape[1]
     small = 16 * heads <= HEAD and arrays[7].shape[1] == HEAD and arrays[11].shape[0] == heads
-    if n % 2 == 0 and n > 2 and whole_tiles and small and tokens.shape[0] * m == SPAN:
+    paired = n % 4 == 0 and n > 4 and m % 2 == 0 and m > 2
+    if paired and whole_tiles and small and tokens.shape[0] * m == SPAN:
         return body(n, m, *arrays)
     return plain_body(*arrays)
 

time: 82.8 us -> 73.7 us (0.89)
  the two profiles are of different devices: /device:TPU:0 before, /device:TPU:17 now
where the time goes in v1:
time: 73.7 us; the launch traced here: 73.5 us
  Pallas kernels  71.8 us (97%)
  local copies, waits for them, and re-layouts  1.67 us (2%)
    pallas_call x1, Pallas kernels, body(): pl.pallas_call(functools.partial(kernel, n, m, heads), out_shape=jax.Shap...  71.8 us
    unnamed x1, local copies, waits for them, and re-layouts  1.67 us

profile of v1, /device:TPU:17, one launch (start us, length us, event | category | flops | bytes accessed | tf_op | source)
XLA Modules:
  0.0 73.5 jit_solution(3180988494762271320)
XLA Ops:
  0.0 71.8 %shard_map.127 = bf16[64,2048]{1,0:T(8,128)(2,1)} custom-call(bf16[64,2048]{1,0:T(8,128)(2,1)} %tok_hbm.1, f32[1,2048]{1,0:T(1,128)} %bitcast.14, bf16[192,256]{1,0:T(8,128)(2,1)} %bitcast.8, bf16[192,256]{1,0:T(8,128)(2,1)} %bitcast.9, bf16[192,256]{1,0:T(8,128)(2,1)} %bitcast.10, bf16[192,256]{1,0:T(8,128)(2,1)} %bitcast.11, bf16[64,256]{1,0:T(8,128)(2,1)} %bitcast.12, ...), custom_call_target="tpu_custom_call" | custom-call | tf_op jit(solution)/shard_map/pallas_call | solution.py:507
  71.8 1.7 %copy.15 = bf16[64,2048]{1,0:T(8,128)(2,1)} copy(bf16[64,2048]{1,0:T(8,128)(2,1)} %shard_map.127) | data formatting | bytes 524288

commit v2 on v1

--- a/solution.py
+++ b/solution.py
@@ -17,6 +17,8 @@
 SPAN = 256
 KEY_SPAN = 256
 LANES = 128
+CUT = 2
+TOKEN_CUT = 2
 HIGH = lax.Precision.HIGHEST
 
 
@@ -51,6 +53,7 @@
     bbuf,
     obuf,
     kvbuf,
+    stbuf,
     state,
     num,
     den,
@@ -63,6 +66,7 @@
     x_fwd,
     x_recv,
     w_send,
+    w_near,
     w_part,
     w_y,
     w_recv,
@@ -70,6 +74,8 @@
     k_y,
     k_part,
     k_recv,
+    st_send,
+    st_recv,
     r_send,
     r_recv,
 ):
@@ -105,10 +111,10 @@
             (tok_hbm, tokens),
             (wk_att_hbm, abuf.at[slot, pl.ds(0, HEAD)]),
             (wv_att_hbm, abuf.at[slot, pl.ds(HEAD, HEAD)]),
-            (wk_ret_hbm, abuf.at[slot, pl.ds(2 * HEAD, width)]),
-            (wv_ret_hbm, abuf.at[slot, pl.ds(2 * HEAD + width, width)]),
-            (wq_att_hbm, bbuf.at[slot, pl.ds(0, width)]),
-            (wq_ret_hbm, bbuf.at[slot, pl.ds(width, width)]),
+            (wq_att_hbm, abuf.at[slot, pl.ds(2 * HEAD, width)]),
+            (wk_ret_hbm, bbuf.at[slot, pl.ds(0, width)]),
+            (wv_ret_hbm, bbuf.at[slot, pl.ds(width, width)]),
+            (wq_ret_hbm, bbuf.at[slot, pl.ds(2 * width, width)]),
             (wo_ret_hbm, obuf.at[slot, pl.ds(0, half_o)]),
             (wo_att_hbm, obuf.at[slot, pl.ds(half_o, wo_att_hbm.shape[0])]),
             (table_hbm.at[pl.ds(pl.multiple_of(q * tok, tok), tok)], table),
@@ -120,7 +126,9 @@
         copy.start()
 
     barrier = pltpu.get_barrier_semaphore()
-    greeted = [across]
+    greeted = [
+        device((zh + i) % nh, zl, 1 - y, x, (c + k) % 2) for i in range(nh) for k in range(2)
+    ]
     for i in reversed(range(nh)):
         for j in reversed(range(2)):
             for k in range(2):
@@ -167,95 +175,146 @@
     pl.semaphore_wait(barrier, len(greeted))
 
     parts = (abuf, bbuf, obuf)
-
-    def half(buf, index, k):
-        length = buf.shape[1] // 2
-        return buf.at[index, pl.ds(pl.multiple_of(k * length, length), length)]
-
-    def scatter(p, i):
+    cut = w_recv.shape[3]
+
+    def chunk(buf, index, k, u):
+        length = buf.shape[1] // (2 * cut)
+        return buf.at[index, pl.ds(pl.multiple_of((k * cut + u) * length, length), length)]
+
+    def scatter_one(p, i, k, u, condition):
         buf = parts[p]
-        for k in (1, 0):
+        core = (c + k) % 2
+        send(
+            chunk(buf, slot, core, u), chunk(buf, s, core, u),
+            w_send.at[p, i, k, u], w_recv.at[p, s, core, u],
+            device((zh + i) % nh, c, y, x, core), condition,
+        )
+
+    def scatter_chip(p):
+        for u in range(cut):
+            scatter_one(p, 0, 1, u, own)
+
+    def scatter_near(p, u):
+        buf = parts[p]
+        for k in range(2):
             core = (c + k) % 2
             send(
-                half(buf, slot, core), half(buf, s, core),
-                w_send.at[p, i, k], w_recv.at[p, s, core],
-                device((zh + i) % nh, c, y, x, core),
-                apart if i == 0 and k == 0 else None,
+                chunk(buf, slot, core, u), chunk(buf, s, core, u),
+                w_near.at[p, k, u], w_recv.at[p, s, core, u],
+                device(zh, c, y, x, core), apart,
             )
 
-    def entry(p, i, j):
+    def scatter_far(p, u):
+        for i in range(1, nh):
+            for k in range(2):
+                scatter_one(p, i, k, u, None)
+
+    def entry(p, i, j, u):
         buf = parts[p]
         index = sp_of((zh + i) % nh, (zl + j) % 2, y)
         here = i == 0 and j == 0
-        spot = half(buf, index, c)
-        receive(spot, w_recv.at[p, index, c], apart if here else None)
-        send(spot, spot, w_y.at[p, i, j], w_recv.at[p, index, c], across)
+        spot = chunk(buf, index, c, u)
+        receive(spot, w_recv.at[p, index, c, u], apart if here else None)
+        send(spot, spot, w_y.at[p, i, j, u], w_recv.at[p, index, c, u], across)
         send(
-            spot, spot, w_part.at[p, i, j, 0], w_recv.at[p, index, c], partner,
+            spot, spot, w_part.at[p, i, j, 0, u], w_recv.at[p, index, c, u], partner,
             own if here else None,
         )
 
-    def beside(p, i, j):
+    def beside(p, i, j, u):
         buf = parts[p]
         index = sp_of((zh + i) % nh, (zl + j) % 2, 1 - y)
-        spot = half(buf, index, c)
-        receive(spot, w_recv.at[p, index, c])
-        send(spot, spot, w_part.at[p, i, j, 1], w_recv.at[p, index, c], partner)
+        spot = chunk(buf, index, c, u)
+        receive(spot, w_recv.at[p, index, c, u])
+        send(spot, spot, w_part.at[p, i, j, 1, u], w_recv.at[p, index, c, u], partner)
 
     def rest(p):
         buf = parts[p]
         for i in range(nh):
             for j in range(2):
                 for k in range(2):
-                    index = sp_of((zh + i) % nh, (zl + j) % 2, (y + k) % 2)
-                    receive(
-                        half(buf, index, 1 - c), w_recv.at[p, index, 1 - c],
-                        apart if i == 0 and j == 0 and k == 0 else None,
-                    )
-
-    order = [(i, j) for i in range(nh) for j in range(2)]
-
-    def rows_of(index):
-        return xbuf.at[pl.ds(pl.multiple_of(index * rows, rows), rows)]
-
-    scatter(0, 0)
-    entry_first = order[0]
-    send(rows_of(piece), rows_of(t), x_send.at[0], x_recv.at[t], device(zh, 1 - zl, y, x, zl))
-    for r in range(1, nx):
+                    for u in range(cut):
+                        index = sp_of((zh + i) % nh, (zl + j) % 2, (y + k) % 2)
+                        receive(
+                            chunk(buf, index, 1 - c, u), w_recv.at[p, index, 1 - c, u],
+                            apart if i == 0 and j == 0 and k == 0 else None,
+                        )
+
+    far = [(i, j) for i in range(1, nh) for j in range(2)]
+    near = (0, 1)
+    pieces = x_recv.shape[1]
+
+    def rows_of(index, u):
+        length = rows // pieces
+        return xbuf.at[pl.ds(pl.multiple_of((index * pieces + u) * length, length), length)]
+
+    def pass_tokens(k, u):
+        index = tp_of(x, (c + k) % 2)
+        spot = rows_of(index, u)
+        receive(spot, x_recv.at[index, u], apart if k == 0 else None)
+        for r in range(1, nx):
+            send(
+                spot, spot, x_fwd.at[r - 1, k, u], x_recv.at[index, u],
+                device(zh, zl, y, (x + r) % nx, c), apart,
+            )
+
+    for u in range(cut):
+        scatter_far(0, u)
+    scatter_chip(0)
+    for u in range(pieces):
         send(
-            rows_of(piece), rows_of(t), x_send.at[1 + r], x_recv.at[t],
-            device(zh, zl, y, (x + r) % nx, zl),
+            rows_of(piece, u), rows_of(t, u), x_send.at[0, u], x_recv.at[t, u],
+            device(zh, 1 - zl, y, x, zl),
         )
-    send(rows_of(piece), rows_of(t), x_send.at[1], x_recv.at[t], device(zh, zl, y, x, zl), apart)
+        for r in range(1, nx):
+            send(
+                rows_of(piece, u), rows_of(t, u), x_send.at[1 + r, u], x_recv.at[t, u],
+                device(zh, zl, y, (x + r) % nx, zl),
+            )
+        send(
+            rows_of(piece, u), rows_of(t, u), x_send.at[1, u], x_recv.at[t, u],
+            device(zh, zl, y, x, zl), apart,
+        )
+    for u in range(cut):
+        scatter_near(0, u)
+    scatter_chip(1)
+    scatter_chip(2)
+    for u in range(cut):
+        scatter_far(1, u)
+        scatter_near(1, u)
     send(
         lbuf.at[0], lbuf.at[1], small_send.at[0], small_recv.at[0],
         device(zh, c, y, x, zl), apart,
     )
     send(gbuf.at[0], gbuf.at[1], small_send.at[1], small_recv.at[1], partner, own)
-    for i in range(1, nh):
-        scatter(0, i)
-    entry(0, *entry_first)
-    for i in range(nh):
-        scatter(1, i)
-
-    def pass_tokens(k):
-        index = tp_of(x, (c + k) % 2)
-        spot = rows_of(index)
-        receive(spot, x_recv.at[index], apart if k == 0 else None)
-        for r in range(1, nx):
-            send(
-                spot, spot, x_fwd.at[r - 1, k], x_recv.at[index],
-                device(zh, zl, y, (x + r) % nx, c), apart,
-            )
-
-    entry(0, *order[1])
-    beside(0, *order[0])
+    for p in range(3):
+        for u in range(cut):
+            entry(p, 0, 0, u)
+    for u in range(cut):
+        beside(0, 0, 0, u)
+    for a in far:
+        entry(0, *a, 0)
     for k in range(2):
-        pass_tokens(k)
-    for a in range(2, len(order)):
-        entry(0, *order[a])
-        beside(0, *order[a - 1])
-    beside(0, *order[-1])
+        pass_tokens(k, 0)
+    for u in range(cut):
+        beside(1, 0, 0, u)
+    for u in range(1, cut):
+        for a in far:
+            entry(0, *a, u)
+    for a in far:
+        beside(0, *a, 0)
+    for u in range(1, pieces):
+        for k in range(2):
+            pass_tokens(k, u)
+    for u in range(cut):
+        entry(0, *near, u)
+    for u in range(1, cut):
+        for a in far:
+            beside(0, *a, u)
+    for a in far:
+        entry(1, *a, 0)
+    for u in range(cut):
+        beside(0, *near, u)
 
     lines = lax.broadcasted_iota(jnp.int32, (tok, tok), 0)
     lanes = lax.broadcasted_iota(jnp.int32, (tok, tok), 1)
@@ -280,8 +339,50 @@
     for r in range(1, nx):
         for k in range(2):
             index = tp_of((x + r) % nx, k)
-            receive(rows_of(index), x_recv.at[index])
+            for u in range(pieces):
+                receive(rows_of(index, u), x_recv.at[index, u])
     rest(0)
+
+    def exchange(buf, e, index, sem, where, condition):
+        send(buf.at[index], buf.at[index], sem, k_recv.at[e, index], where, condition)
+
+    def arrive(buf, e, index, condition):
+        receive(buf.at[index], k_recv.at[e, index], condition)
+
+    def exchange_send(buf, e):
+        for i in range(1, nh):
+            exchange(
+                buf, e, q, k_send.at[e, i - 1], device((zh + i) % nh, zl, y, x, c), zh + i < nh
+            )
+        exchange(buf, e, q, k_y.at[e, 0], across, c + y < 2)
+        exchange(buf, e, q, k_part.at[e, 0, 0], partner, c == 0)
+
+    def exchange_across(buf, e):
+        index = sp_of(zh, c, 1 - y)
+        arrive(buf, e, index, c <= y)
+        exchange(buf, e, index, k_part.at[e, 0, 1], partner, c == 0)
+
+    def exchange_part(buf, e):
+        for k in range(2):
+            arrive(buf, e, sp_of(zh, 1 - c, (y + k) % 2), c == 1)
+
+    def exchange_far(buf, e):
+        for i in range(1, nh):
+            index = sp_of((zh + nh - i) % nh, c, y)
+            arrive(buf, e, index, zh >= i)
+            exchange(buf, e, index, k_y.at[e, i], across, zh >= i)
+            exchange(buf, e, index, k_part.at[e, i, 0], partner, zh >= i)
+
+    def exchange_far_across(buf, e):
+        for i in range(1, nh):
+            index = sp_of((zh + nh - i) % nh, c, 1 - y)
+            arrive(buf, e, index, zh >= i)
+            exchange(buf, e, index, k_part.at[e, i, 1], partner, zh >= i)
+
+    def exchange_far_part(buf, e):
+        for i in range(1, nh):
+            for k in range(2):
+                arrive(buf, e, sp_of((zh + nh - i) % nh, 1 - c, (y + k) % 2), zh >= i)
 
     def rope(field):
         first, second = field[:, : HEAD // 2], field[:, HEAD // 2 :]
@@ -296,10 +397,64 @@
         )
 
     proj = project(abuf)
-    pair = proj[:, : 2 * HEAD].astype(BF16)
+    kvbuf[q] = proj[:, : 2 * HEAD].astype(BF16)
+    exchange_send(kvbuf, 0)
+    for u in range(cut):
+        scatter_far(2, u)
+        scatter_near(2, u)
+    queries = [
+        (proj[:, (2 + h) * HEAD : (3 + h) * HEAD] * HEAD ** (-0.5)).astype(BF16)
+        for h in range(heads)
+    ]
+
+    def attend(index, masked):
+        block = kvbuf[index]
+        key, val = block[:, :HEAD], block[:, HEAD:]
+        gates = gbuf[pick, :, pl.ds(pl.multiple_of(index * tok, tok), tok)]
+        for h in range(heads):
+            logits = dot(queries[h], key, ((1,), (1,)))
+            logits = logits + gate_col[:, h : h + 1] - gates[h : h + 1, :]
+            if masked:
+                logits = jnp.where(causal, logits, -jnp.inf)
+            weights = jnp.exp(logits)
+            den[h] += jnp.broadcast_to(jnp.sum(weights, axis=-1, keepdims=True), (tok, HEAD))
+            num[h] += dot(weights.astype(BF16), val)
+
+    den[...] = jnp.zeros_like(den)
+    num[...] = jnp.zeros_like(num)
+    attend(q, True)
+    for u in range(1, cut):
+        for a in far:
+            entry(1, *a, u)
+    entry(1, *near, 0)
+    exchange_across(kvbuf, 0)
+    for a in far:
+        beside(1, *a, 0)
+    for u in range(cut):
+        beside(2, 0, 0, u)
+    exchange_part(kvbuf, 0)
+    index = sp_of(zh, 0, 0)
+    pl.when(index < q)(functools.partial(attend, index, False))
+    for u in range(1, cut):
+        entry(1, *near, u)
+    exchange_far(kvbuf, 0)
+    pl.when(index + 1 < q)(functools.partial(attend, index + 1, False))
+    for u in range(1, cut):
+        for a in far:
+            beside(1, *a, u)
+    beside(1, *near, 0)
+    pl.when(index + 2 < q)(functools.partial(attend, index + 2, False))
+    exchange_far_across(kvbuf, 0)
+    for u in range(1, cut):
+        beside(1, *near, u)
+    for a in far:
+        entry(2, *a, 0)
+    rest(1)
+
+    proj = project(bbuf)
     keys, vals, updates, marks = [], [], [], []
     for h in range(heads):
-        base = 2 * HEAD + h * HEAD
+        base = h * HEAD
         key = rope(proj[:, base : base + HEAD]).astype(BF16)
         val = proj[:, base + width : base + width + HEAD].astype(BF16)
         column = within[:, h : h + 1]
@@ -312,118 +467,62 @@
         marks.append(jnp.broadcast_to(low, (8, HEAD)))
         keys.append(key)
         vals.append(val)
-    kvbuf[q, :tok, :] = pair
     marks.append(jnp.zeros((HEAD - 16 * heads, HEAD), F32))
     blocks = updates + [jnp.concatenate(marks, axis=0)]
     if len(blocks) % 2:
         blocks.append(jnp.zeros((HEAD, HEAD), F32))
     for k in range(0, len(blocks), 2):
         both = jnp.concatenate(blocks[k : k + 2], axis=1).astype(BF16)
-        kvbuf[q, tok + k // 2 * HEAD : tok + (k // 2 + 1) * HEAD, :] = both
+        stbuf[q, k // 2 * HEAD : (k // 2 + 1) * HEAD, :] = both
 
     def piece_of(index, k):
         spot = slice(k % 2 * HEAD, (k % 2 + 1) * HEAD)
-        return kvbuf[index, tok + k // 2 * HEAD : tok + (k // 2 + 1) * HEAD, spot].astype(F32)
-
-    def share(index, sem, where, condition=None):
-        send(kvbuf.at[index], kvbuf.at[index], sem, k_recv.at[index], where, condition)
-
-    def arrive(index, condition=None):
-        receive(kvbuf.at[index], k_recv.at[index], condition)
-
+        return stbuf[index, k // 2 * HEAD : (k // 2 + 1) * HEAD, spot].astype(F32)
+
+    for i in range(nh):
+        for l in range(2):
+            for e in range(2):
+                if i or l or e:
+                    index = sp_of((zh + i) % nh, (c + e) % 2, (y + l) % 2)
+                    send(
+                        stbuf.at[q], stbuf.at[q], st_send.at[i, l, e], st_recv.at[q],
+                        device((zh + i) % nh, zl, (y + l) % 2, x, (c + e) % 2), index > q,
+                    )
+    exchange_far_part(kvbuf, 0)
+    steps = [(entry, near, 0)]
+    steps += [(entry, a, u) for u in range(1, cut) for a in far]
+    steps += [(entry, near, u) for u in range(1, cut)]
+    steps += [(beside, a, 0) for a in far]
     for i in range(1, nh):
-        share(q, k_send.at[i - 1], device((zh + i) % nh, zl, y, x, c), zh + i < nh)
-    share(q, k_y.at[0], across, c + y < 2)
-    share(q, k_part.at[0, 0], partner, c == 0)
-    for i in range(nh):
-        scatter(2, i)
-
-    for a in range(len(order)):
-        entry(1, *order[a])
-        if a:
-            beside(1, *order[a - 1])
-        if a == 0:
-            index = sp_of(zh, c, 1 - y)
-            arrive(index, c <= y)
-            share(index, k_part.at[0, 1], partner, c == 0)
-    for i in range(1, nh):
-        index = sp_of((zh + nh - i) % nh, c, y)
-        arrive(index, zh >= i)
-        share(index, k_y.at[i], across, zh >= i)
-        share(index, k_part.at[i, 0], partner, zh >= i)
-    beside(1, *order[-1])
-    entry(2, *order[0])
-    for i in range(1, nh):
-        index = sp_of((zh + nh - i) % nh, c, 1 - y)
-        arrive(index, zh >= i)
-        share(index, k_part.at[i, 1], partner, zh >= i)
-    rest(1)
-
-    projq = project(bbuf)
-    entry(2, *order[1])
-    beside(2, *order[0])
+        for j in range(4):
+            index = sp_of((zh + nh - i) % nh, 0, 0) + j
+            pl.when(zh >= i)(functools.partial(attend, index, False))
+            for call, a, u in steps[:1]:
+                call(2, *a, u)
+            steps = steps[1:]
     local, lifts = [], []
     for h in range(heads):
-        base = width + h * HEAD
-        query = (rope(projq[:, base : base + HEAD]) * HEAD ** (-0.5)).astype(BF16)
+        base = 2 * width + h * HEAD
+        query = (rope(proj[:, base : base + HEAD]) * HEAD ** (-0.5)).astype(BF16)
         column = within[:, h : h + 1]
         gap = jnp.where(causal, column - turned[h : h + 1, :], 0.0)
         scores = dot(query, keys[h], ((1,), (1,)))
         weights = jnp.where(causal, scores * jnp.exp(gap), 0.0).astype(BF16)
         local.append(dot(weights, vals[h]))
         lifts.append((query.astype(F32) * jnp.exp(column)).astype(BF16))
-
-    queries = [
-        (projq[:, h * HEAD : (h + 1) * HEAD] * HEAD ** (-0.5)).astype(BF16) for h in range(heads)
-    ]
-
-    def attend(index, masked):
-        block = kvbuf[index, :tok, :]
-        key, val = block[:, :HEAD], block[:, HEAD:]
-        gates = gbuf[pick, :, pl.ds(pl.multiple_of(index * tok, tok), tok)]
-        for h in range(heads):
-            logits = dot(queries[h], key, ((1,), (1,)))
-            logits = logits + gate_col[:, h : h + 1] - gates[h : h + 1, :]
-            if masked:
-                logits = jnp.where(causal, logits, -jnp.inf)
-            weights = jnp.exp(logits)
-            den[h] += jnp.broadcast_to(jnp.sum(weights, axis=-1, keepdims=True), (tok, HEAD))
-            num[h] += dot(weights.astype(BF16), val)
-
-    den[...] = jnp.zeros_like(den)
-    num[...] = jnp.zeros_like(num)
+    for call, a, u in steps:
+        call(2, *a, u)
+    for j in range(n - 1):
+        receive(stbuf.at[j], st_recv.at[j], q > j)
     state[...] = jnp.zeros_like(state)
-    attend(q, True)
-    entry(2, *order[2])
-    beside(2, *order[1])
-    for k in range(2):
-        arrive(sp_of(zh, 1 - c, (y + k) % 2), c == 1)
-    for i in range(1, nh):
-        for k in range(2):
-            arrive(sp_of((zh + nh - i) % nh, 1 - c, (y + k) % 2), zh >= i)
-    pending = [(entry, a) for a in order[3:]]
-    after = [(beside, a) for a in order[2:]]
-    steps = []
-    for a in range(len(after)):
-        if a < len(pending):
-            steps.append(pending[a])
-        steps.append(after[a])
     for j in range(n - 1):
         def earlier(j=j):
             marked = piece_of(j, heads)
             for h in range(heads):
                 total = marked[16 * h : 16 * h + 1] + marked[16 * h + 8 : 16 * h + 9]
                 state[h] = jnp.exp(total) * state[h] + piece_of(j, h)
-            attend(j, False)
 
         pl.when(q > j)(earlier)
-        if j % 2 == 0 and steps:
-            call, a = steps.pop(0)
-            call(2, *a)
-    for call, a in steps:
-        call(2, *a)
-    rest(2)
-
     retained, attended = [], []
     for h in range(heads):
         raw = local[h] + dot(lifts[h], state[h].astype(BF16))
@@ -432,6 +531,12 @@
         retained.append(((raw - centre) * lax.rsqrt(spread + EPS)).astype(BF16))
         attended.append((num[h] / den[h]).astype(BF16))
     mixed = jnp.concatenate(retained + attended, axis=-1)
+    beside(2, *near, 0)
+    for u in range(1, cut):
+        for a in far:
+            beside(2, *a, u)
+        beside(2, *near, u)
+    rest(2)
 
     columns = obuf.shape[2]
     group = 2
@@ -496,11 +601,11 @@
     inverse = np.float32(THETA) ** (-np.arange(half, dtype=np.float32) / np.float32(half))
     angles = np.arange(n * tok, dtype=np.float32)[:, None] * inverse[None, :]
     table = np.concatenate([np.cos(angles), np.sin(angles)], axis=1).astype(np.float32)
-    wide_a = 2 * HEAD + 2 * heads * HEAD
-    wide_b = 2 * heads * HEAD
+    wide_a = 2 * HEAD + heads * HEAD
+    wide_b = 3 * heads * HEAD
     deep = w_key_ret.shape[0]
     deep_o = w_out_ret.shape[0] + w_out_att.shape[0]
-    tall = tok + (heads // 2 + 1) * HEAD
+    tall = (heads // 2 + 1) * HEAD
     hbm = pl.BlockSpec(memory_space=pl.ANY)
     vmem = pl.BlockSpec(memory_space=pltpu.VMEM)
     dma = pltpu.SemaphoreType.DMA
@@ -518,6 +623,7 @@
             pltpu.VMEM((n + 1, wide_a, deep), BF16),
             pltpu.VMEM((n + 1, wide_b, deep), BF16),
             pltpu.VMEM((n + 1, deep_o, w_out_ret.shape[1]), BF16),
+            pltpu.VMEM((n, tok, 2 * HEAD), BF16),
             pltpu.VMEM((n, tall, 2 * HEAD), BF16),
             pltpu.VMEM((heads, HEAD, HEAD), F32),
             pltpu.VMEM((heads, tok, HEAD), F32),
@@ -527,16 +633,19 @@
             dma((12,)),
             dma((2,)),
             dma((2,)),
-            dma((1 + nx,)),
-            dma((nx - 1, 2)),
-            dma((m,)),
-            dma((3, nh, 2)),
-            dma((3, nh, 2, 2)),
-            dma((3, nh, 2)),
-            dma((3, n, 2)),
-            dma((nh - 1,)),
-            dma((nh,)),
-            dma((nh, 2)),
+            dma((1 + nx, TOKEN_CUT)),
+            dma((nx - 1, 2, TOKEN_CUT)),
+            dma((m, TOKEN_CUT)),
+            dma((3, nh, 2, CUT)),
+            dma((3, 2, CUT)),
+            dma((3, nh, 2, 2, CUT)),
+            dma((3, nh, 2, CUT)),
+            dma((3, n, 2, CUT)),
+            dma((1, nh - 1)),
+            dma((1, nh)),
+            dma((1, nh, 2)),
+            dma((1, n)),
+            dma((nh, 2, 2)),
             dma((n,)),
             dma((n // 2, nx, 2)),
             dma((n // 2, m)),

time: 73.7 us -> 69.3 us (0.940)
  Pallas kernels: 71.8 us -> 67.4 us
    pallas_call x1, Pallas kernels: 71.8 us -> 67.4 us  [body(): pl.pallas_call(functools.partial(kernel, n, m, heads), out_shape=jax.Shap...]
where the time goes in v2:
time: 69.3 us; the launch traced here: 69 us
  Pallas kernels  67.4 us (97%)
  local copies, waits for them, and re-layouts  1.67 us (2%)
    pallas_call x1, Pallas kernels, body(): pl.pallas_call(functools.partial(kernel, n, m, heads), out_shape=jax.Shap...  67.4 us
    unnamed x1, local copies, waits for them, and re-layouts  1.67 us

profile of v2, /device:TPU:17, one launch (start us, length us, event | category | flops | bytes accessed | tf_op | source)
XLA Modules:
  0.0 69.0 jit_solution(14019951847518784573)
XLA Ops:
  0.0 67.4 %shard_map.127 = bf16[64,2048]{1,0:T(8,128)(2,1)} custom-call(bf16[64,2048]{1,0:T(8,128)(2,1)} %tok_hbm.1, f32[1,2048]{1,0:T(1,128)} %bitcast.14, bf16[192,256]{1,0:T(8,128)(2,1)} %bitcast.8, bf16[192,256]{1,0:T(8,128)(2,1)} %bitcast.9, bf16[192,256]{1,0:T(8,128)(2,1)} %bitcast.10, bf16[192,256]{1,0:T(8,128)(2,1)} %bitcast.11, bf16[64,256]{1,0:T(8,128)(2,1)} %bitcast.12, ...), custom_call_target="tpu_custom_call" | custom-call | tf_op jit(solution)/shard_map/pallas_call | solution.py:612
  67.4 1.7 %copy.15 = bf16[64,2048]{1,0:T(8,128)(2,1)} copy(bf16[64,2048]{1,0:T(8,128)(2,1)} %shard_map.127) | data formatting | bytes 524288

commit v3 on v2

--- a/solution.py
+++ b/solution.py
@@ -17,7 +17,8 @@
 SPAN = 256
 KEY_SPAN = 256
 LANES = 128
-CUT = 2
+CUTS = (2, 2, 1, 2)
+LOG2E = float(np.log2(np.e))
 TOKEN_CUT = 2
 HIGH = lax.Precision.HIGHEST
 
@@ -51,12 +52,14 @@
     xbuf,
     abuf,
     bbuf,
+    cbuf,
     obuf,
     kvbuf,
     stbuf,
     state,
     num,
-    den,
+    qbuf,
+    cbuf_gate,
     outbuf,
     rsbuf,
     load,
@@ -75,6 +78,7 @@
     k_part,
     k_recv,
     st_send,
+    st_fwd,
     st_recv,
     r_send,
     r_recv,
@@ -114,7 +118,7 @@
             (wq_att_hbm, abuf.at[slot, pl.ds(2 * HEAD, width)]),
             (wk_ret_hbm, bbuf.at[slot, pl.ds(0, width)]),
             (wv_ret_hbm, bbuf.at[slot, pl.ds(width, width)]),
-            (wq_ret_hbm, bbuf.at[slot, pl.ds(2 * width, width)]),
+            (wq_ret_hbm, cbuf.at[slot]),
             (wo_ret_hbm, obuf.at[slot, pl.ds(0, half_o)]),
             (wo_att_hbm, obuf.at[slot, pl.ds(half_o, wo_att_hbm.shape[0])]),
             (table_hbm.at[pl.ds(pl.multiple_of(q * tok, tok), tok)], table),
@@ -174,71 +178,73 @@
         copy.wait()
     pl.semaphore_wait(barrier, len(greeted))
 
-    parts = (abuf, bbuf, obuf)
-    cut = w_recv.shape[3]
-
-    def chunk(buf, index, k, u):
-        length = buf.shape[1] // (2 * cut)
-        return buf.at[index, pl.ds(pl.multiple_of((k * cut + u) * length, length), length)]
+    parts = (abuf, bbuf, cbuf, obuf)
+    cuts = CUTS
+
+    def chunk(p, index, k, u):
+        length = parts[p].shape[1] // (2 * cuts[p])
+        start = pl.multiple_of((k * cuts[p] + u) * length, length)
+        return parts[p].at[index, pl.ds(start, length)]
 
     def scatter_one(p, i, k, u, condition):
-        buf = parts[p]
         core = (c + k) % 2
         send(
-            chunk(buf, slot, core, u), chunk(buf, s, core, u),
+            chunk(p, slot, core, u), chunk(p, s, core, u),
             w_send.at[p, i, k, u], w_recv.at[p, s, core, u],
             device((zh + i) % nh, c, y, x, core), condition,
         )
 
     def scatter_chip(p):
-        for u in range(cut):
+        for u in range(cuts[p]):
             scatter_one(p, 0, 1, u, own)
 
     def scatter_near(p, u):
-        buf = parts[p]
         for k in range(2):
             core = (c + k) % 2
             send(
-                chunk(buf, slot, core, u), chunk(buf, s, core, u),
+                chunk(p, slot, core, u), chunk(p, s, core, u),
                 w_near.at[p, k, u], w_recv.at[p, s, core, u],
                 device(zh, c, y, x, core), apart,
             )
 
-    def scatter_far(p, u):
+    def scatter_far(p, u, condition=None):
         for i in range(1, nh):
             for k in range(2):
-                scatter_one(p, i, k, u, None)
-
-    def entry(p, i, j, u):
-        buf = parts[p]
+                scatter_one(p, i, k, u, condition)
+
+    middle = zl != zh % 2
+    outer = zl == zh % 2
+
+    def entry(p, i, j, u, condition=None):
         index = sp_of((zh + i) % nh, (zl + j) % 2, y)
         here = i == 0 and j == 0
-        spot = chunk(buf, index, c, u)
-        receive(spot, w_recv.at[p, index, c, u], apart if here else None)
-        send(spot, spot, w_y.at[p, i, j, u], w_recv.at[p, index, c, u], across)
+        spot = chunk(p, index, c, u)
+        receive(spot, w_recv.at[p, index, c, u], apart if here else condition)
+        send(spot, spot, w_y.at[p, i, j, u], w_recv.at[p, index, c, u], across, condition)
         send(
             spot, spot, w_part.at[p, i, j, 0, u], w_recv.at[p, index, c, u], partner,
-            own if here else None,
+            own if here else condition,
         )
 
     def beside(p, i, j, u):
-        buf = parts[p]
         index = sp_of((zh + i) % nh, (zl + j) % 2, 1 - y)
-        spot = chunk(buf, index, c, u)
+        spot = chunk(p, index, c, u)
         receive(spot, w_recv.at[p, index, c, u])
         send(spot, spot, w_part.at[p, i, j, 1, u], w_recv.at[p, index, c, u], partner)
 
+    def ready(p, i, j, l):
+        index = sp_of((zh + i) % nh, (zl + j) % 2, (y + l) % 2)
+        for u in range(cuts[p]):
+            receive(
+                chunk(p, index, 1 - c, u), w_recv.at[p, index, 1 - c, u],
+                apart if i == 0 and j == 0 and l == 0 else None,
+            )
+
     def rest(p):
-        buf = parts[p]
         for i in range(nh):
             for j in range(2):
-                for k in range(2):
-                    for u in range(cut):
-                        index = sp_of((zh + i) % nh, (zl + j) % 2, (y + k) % 2)
-                        receive(
-                            chunk(buf, index, 1 - c, u), w_recv.at[p, index, 1 - c, u],
-                            apart if i == 0 and j == 0 and k == 0 else None,
-                        )
+                for l in range(2):
+                    ready(p, i, j, l)
 
     far = [(i, j) for i in range(1, nh) for j in range(2)]
     near = (0, 1)
@@ -258,7 +264,12 @@
                 device(zh, zl, y, (x + r) % nx, c), apart,
             )
 
-    for u in range(cut):
+    send(
+        lbuf.at[0], lbuf.at[1], small_send.at[0], small_recv.at[0],
+        device(zh, c, y, x, zl), apart,
+    )
+    send(gbuf.at[0], gbuf.at[1], small_send.at[1], small_recv.at[1], partner, own)
+    for u in range(cuts[0]):
         scatter_far(0, u)
     scatter_chip(0)
     for u in range(pieces):
@@ -275,47 +286,17 @@
             rows_of(piece, u), rows_of(t, u), x_send.at[1, u], x_recv.at[t, u],
             device(zh, zl, y, x, zl), apart,
         )
-    for u in range(cut):
+    for u in range(cuts[0]):
         scatter_near(0, u)
-    scatter_chip(1)
-    scatter_chip(2)
-    for u in range(cut):
-        scatter_far(1, u)
-        scatter_near(1, u)
-    send(
-        lbuf.at[0], lbuf.at[1], small_send.at[0], small_recv.at[0],
-        device(zh, c, y, x, zl), apart,
-    )
-    send(gbuf.at[0], gbuf.at[1], small_send.at[1], small_recv.at[1], partner, own)
-    for p in range(3):
-        for u in range(cut):
+    for p in range(1, 4):
+        scatter_chip(p)
+    for p in range(1, 3):
+        for u in range(cuts[p]):
+            scatter_far(p, u)
+            scatter_near(p, u)
+    for p in range(4):
+        for u in range(cuts[p]):
             entry(p, 0, 0, u)
-    for u in range(cut):
-        beside(0, 0, 0, u)
-    for a in far:
-        entry(0, *a, 0)
-    for k in range(2):
-        pass_tokens(k, 0)
-    for u in range(cut):
-        beside(1, 0, 0, u)
-    for u in range(1, cut):
-        for a in far:
-            entry(0, *a, u)
-    for a in far:
-        beside(0, *a, 0)
-    for u in range(1, pieces):
-        for k in range(2):
-            pass_tokens(k, u)
-    for u in range(cut):
-        entry(0, *near, u)
-    for u in range(1, cut):
-        for a in far:
-            beside(0, *a, u)
-    for a in far:
-        entry(1, *a, 0)
-    for u in range(cut):
-        beside(0, *near, u)
-
     lines = lax.broadcasted_iota(jnp.int32, (tok, tok), 0)
     lanes = lax.broadcasted_iota(jnp.int32, (tok, tok), 1)
     causal = lines >= lanes
@@ -336,6 +317,37 @@
     ).T
     cosine, sine = table[:, : HEAD // 2], table[:, HEAD // 2 :]
 
+    for u in range(cuts[0]):
+        beside(0, 0, 0, u)
+    for a in far:
+        entry(0, *a, 0)
+    for k in range(2):
+        pass_tokens(k, 0)
+    for u in range(cuts[1]):
+        beside(1, 0, 0, u)
+    for u in range(1, cuts[0]):
+        for a in far:
+            entry(0, *a, u)
+    for a in far:
+        beside(0, *a, 0)
+    for u in range(1, pieces):
+        for k in range(2):
+            pass_tokens(k, u)
+    for u in range(cuts[0]):
+        entry(0, *near, u)
+    for a in far:
+        entry(1, *a, 0, middle)
+    for u in range(1, cuts[0]):
+        for a in far:
+            beside(0, *a, u)
+    for p in range(2, 4):
+        for u in range(cuts[p]):
+            beside(p, 0, 0, u)
+    for u in range(cuts[0]):
+        beside(0, *near, u)
+    for a in far:
+        entry(1, *a, 0, outer)
+
     for r in range(1, nx):
         for k in range(2):
             index = tp_of((x + r) % nx, k)
@@ -399,56 +411,69 @@
     proj = project(abuf)
     kvbuf[q] = proj[:, : 2 * HEAD].astype(BF16)
     exchange_send(kvbuf, 0)
-    for u in range(cut):
-        scatter_far(2, u)
-        scatter_near(2, u)
-    queries = [
-        (proj[:, (2 + h) * HEAD : (3 + h) * HEAD] * HEAD ** (-0.5)).astype(BF16)
-        for h in range(heads)
-    ]
-
-    def attend(index, masked):
-        block = kvbuf[index]
-        key, val = block[:, :HEAD], block[:, HEAD:]
-        gates = gbuf[pick, :, pl.ds(pl.multiple_of(index * tok, tok), tok)]
-        for h in range(heads):
-            logits = dot(queries[h], key, ((1,), (1,)))
-            logits = logits + gate_col[:, h : h + 1] - gates[h : h + 1, :]
-            if masked:
-                logits = jnp.where(causal, logits, -jnp.inf)
-            weights = jnp.exp(logits)
-            den[h] += jnp.broadcast_to(jnp.sum(weights, axis=-1, keepdims=True), (tok, HEAD))
-            num[h] += dot(weights.astype(BF16), val)
-
-    den[...] = jnp.zeros_like(den)
-    num[...] = jnp.zeros_like(num)
-    attend(q, True)
-    for u in range(1, cut):
+    scatter_far(3, 0)
+    scatter_near(3, 0)
+    for u in range(1, cuts[3]):
+        scatter_far(3, u, zh == nh - 1)
+        scatter_near(3, u)
+    wide = heads * tok
+    zeros = jnp.zeros((tok, HEAD), F32)
+    for h in range(heads):
+        query = proj[:, (2 + h) * HEAD : (3 + h) * HEAD] * (HEAD ** (-0.5) * LOG2E)
+        qbuf[h * tok : (h + 1) * tok, :] = jnp.concatenate([query, zeros], axis=1).astype(BF16)
+        cbuf_gate[h * tok : (h + 1) * tok, :] = jnp.broadcast_to(
+            gate_col[:, h : h + 1] * LOG2E, (tok, LANES)
+        )
+    low_lanes = lax.broadcasted_iota(jnp.int32, (tok, 2 * HEAD), 1) < HEAD
+
+    def attend(indices, masked=False):
+        total = None if masked else num[...]
+        for index in indices:
+            block = kvbuf[index]
+            values = jnp.where(low_lanes, jnp.ones_like(block), block)
+            gates = gbuf[pick, :, pl.ds(pl.multiple_of(index * tok, tok), tok)] * LOG2E
+            logits = dot(qbuf[...], block, ((1,), (1,)))
+            column = cbuf_gate[...]
+            column = jnp.concatenate([column] * (tok // LANES), axis=1)
+            pieces_ = []
+            for h in range(heads):
+                part = slice(h * tok, (h + 1) * tok)
+                shifted = logits[part] + column[part] - gates[h : h + 1, :]
+                if masked:
+                    shifted = jnp.where(causal, shifted, -jnp.inf)
+                pieces_.append(jnp.exp2(shifted).astype(BF16))
+            term = dot(jnp.concatenate(pieces_, axis=0), values)
+            total = term if total is None else total + term
+        num[...] = total
+
+    for u in range(1, cuts[1]):
         for a in far:
             entry(1, *a, u)
-    entry(1, *near, 0)
-    exchange_across(kvbuf, 0)
+    attend([q], True)
     for a in far:
         beside(1, *a, 0)
-    for u in range(cut):
-        beside(2, 0, 0, u)
+    for u in range(cuts[1]):
+        entry(1, *near, u)
+    exchange_across(kvbuf, 0)
     exchange_part(kvbuf, 0)
     index = sp_of(zh, 0, 0)
-    pl.when(index < q)(functools.partial(attend, index, False))
-    for u in range(1, cut):
-        entry(1, *near, u)
+    pl.when(index < q)(functools.partial(attend, [index]))
     exchange_far(kvbuf, 0)
-    pl.when(index + 1 < q)(functools.partial(attend, index + 1, False))
-    for u in range(1, cut):
+    pl.when(index + 1 < q)(functools.partial(attend, [index + 1]))
+    for u in range(1, cuts[1]):
         for a in far:
             beside(1, *a, u)
-    beside(1, *near, 0)
-    pl.when(index + 2 < q)(functools.partial(attend, index + 2, False))
+    for u in range(cuts[2]):
+        for a in far:
+            entry(2, *a, u)
+    pl.when(index + 2 < q)(functools.partial(attend, [index + 2]))
+    for u in range(cuts[1]):
+        beside(1, *near, u)
+    for u in range(cuts[2]):
+        entry(2, *near, u)
     exchange_far_across(kvbuf, 0)
-    for u in range(1, cut):
-        beside(1, *near, u)
     for a in far:
-        entry(2, *a, 0)
+        entry(3, *a, 0)
     rest(1)
 
     proj = project(bbuf)
@@ -479,41 +504,74 @@
         spot = slice(k % 2 * HEAD, (k % 2 + 1) * HEAD)
         return stbuf[index, k // 2 * HEAD : (k // 2 + 1) * HEAD, spot].astype(F32)
 
-    for i in range(nh):
+    for i in range(1, nh):
+        send(
+            stbuf.at[q], stbuf.at[q], st_send.at[i, 0, 0], st_recv.at[q],
+            device((zh + i) % nh, zl, y, x, c), zh + i < nh,
+        )
+    for l in range(2):
+        for e in range(2):
+            if l or e:
+                index = sp_of(zh, (c + e) % 2, (y + l) % 2)
+                send(
+                    stbuf.at[q], stbuf.at[q], st_send.at[0, l, e], st_recv.at[q],
+                    device(zh, zl, (y + l) % 2, x, (c + e) % 2), index > q,
+                )
+    for u in range(1, cuts[3]):
+        scatter_far(3, u, zh < nh - 1)
+    for u in range(cuts[2]):
+        for a in far:
+            beside(2, *a, u)
+        beside(2, *near, u)
+    entry(3, *near, 0)
+    rest(2)
+
+    for i in range(1, nh):
+        index = sp_of((zh + nh - i) % nh, c, y)
+        receive(stbuf.at[index], st_recv.at[index], zh >= i)
         for l in range(2):
             for e in range(2):
-                if i or l or e:
-                    index = sp_of((zh + i) % nh, (c + e) % 2, (y + l) % 2)
+                if l or e:
                     send(
-                        stbuf.at[q], stbuf.at[q], st_send.at[i, l, e], st_recv.at[q],
-                        device((zh + i) % nh, zl, (y + l) % 2, x, (c + e) % 2), index > q,
+                        stbuf.at[index], stbuf.at[index], st_fwd.at[i, l, e], st_recv.at[index],
+                        device(zh, zl, (y + l) % 2, x, (c + e) % 2), zh >= i,
                     )
-    exchange_far_part(kvbuf, 0)
-    steps = [(entry, near, 0)]
-    steps += [(entry, a, u) for u in range(1, cut) for a in far]
-    steps += [(entry, near, u) for u in range(1, cut)]
-    steps += [(beside, a, 0) for a in far]
-    for i in range(1, nh):
-        for j in range(4):
-            index = sp_of((zh + nh - i) % nh, 0, 0) + j
-            pl.when(zh >= i)(functools.partial(attend, index, False))
-            for call, a, u in steps[:1]:
-                call(2, *a, u)
-            steps = steps[1:]
+    proj = project(cbuf)
     local, lifts = [], []
     for h in range(heads):
-        base = 2 * width + h * HEAD
-        query = (rope(proj[:, base : base + HEAD]) * HEAD ** (-0.5)).astype(BF16)
+        query = (rope(proj[:, h * HEAD : (h + 1) * HEAD]) * HEAD ** (-0.5)).astype(BF16)
         column = within[:, h : h + 1]
         gap = jnp.where(causal, column - turned[h : h + 1, :], 0.0)
         scores = dot(query, keys[h], ((1,), (1,)))
         weights = jnp.where(causal, scores * jnp.exp(gap), 0.0).astype(BF16)
         local.append(dot(weights, vals[h]))
         lifts.append((query.astype(F32) * jnp.exp(column)).astype(BF16))
+    exchange_far_part(kvbuf, 0)
+    steps = [(beside, near, 0)]
+    steps += [(entry, a, u) for u in range(1, cuts[3]) for a in far]
+    steps += [(entry, near, u) for u in range(1, cuts[3])]
+    for i in range(1, nh):
+        index = sp_of((zh + nh - i) % nh, 0, 0)
+        for half in range(2):
+            pl.when(zh >= i)(
+                functools.partial(attend, [index + 2 * half, index + 2 * half + 1])
+            )
+            for call, a, u in steps[:1]:
+                call(3, *a, u)
+            steps = steps[1:]
     for call, a, u in steps:
-        call(2, *a, u)
-    for j in range(n - 1):
-        receive(stbuf.at[j], st_recv.at[j], q > j)
+        call(3, *a, u)
+    for i in range(1, nh):
+        for l in range(2):
+            for e in range(2):
+                if l or e:
+                    index = sp_of((zh + nh - i) % nh, (c + e) % 2, (y + l) % 2)
+                    receive(stbuf.at[index], st_recv.at[index], zh >= i)
+    for l in range(2):
+        for e in range(2):
+            if l or e:
+                index = sp_of(zh, (c + e) % 2, (y + l) % 2)
+                receive(stbuf.at[index], st_recv.at[index], index < q)
     state[...] = jnp.zeros_like(state)
     for j in range(n - 1):
         def earlier(j=j):
@@ -529,50 +587,60 @@
         centre = jnp.mean(raw, axis=-1, keepdims=True)
         spread = jnp.mean(jnp.square(raw - centre), axis=-1, keepdims=True)
         retained.append(((raw - centre) * lax.rsqrt(spread + EPS)).astype(BF16))
-        attended.append((num[h] / den[h]).astype(BF16))
+        both = num[h * tok : (h + 1) * tok, :]
+        attended.append((both[:, HEAD:] / both[:, :HEAD]).astype(BF16))
     mixed = jnp.concatenate(retained + attended, axis=-1)
-    beside(2, *near, 0)
-    for u in range(1, cut):
-        for a in far:
-            beside(2, *a, u)
-        beside(2, *near, u)
-    rest(2)
-
-    columns = obuf.shape[2]
-    group = 2
-    for part in range(n // group):
-        for k in range(part * group, part * group + group):
-            term = dot(mixed, obuf[k]).astype(BF16)
-            outbuf[:, :, k * columns : (k + 1) * columns] = term.reshape(m, rows, columns)
-        span = pl.ds(part * group * columns, group * columns)
+    order = [(i, j) for i in range(nh) for j in range(2)]
+
+    def produce(i, j, l):
+        index = sp_of((zh + i) % nh, (zl + j) % 2, (y + l) % 2)
+        ready(3, i, j, l)
+        outbuf[index] = dot(mixed, obuf[index]).astype(BF16)
         for r in reversed(range(nx)):
             for k in range(2):
-                index = tp_of((x + r) % nx, (c + k) % 2)
+                where = tp_of((x + r) % nx, (c + k) % 2)
+                rows_there = pl.ds(pl.multiple_of(where * rows, rows), rows)
                 send(
-                    outbuf.at[index, :, span], rsbuf.at[g, :, span],
-                    r_send.at[part, r, k], r_recv.at[part, g],
+                    outbuf.at[index, rows_there], rsbuf.at[g, index],
+                    r_send.at[index, r, k], r_recv.at[index, g],
                     device(zh, c, y, (x + r) % nx, (c + k) % 2),
                     apart if r == 0 and k == 0 else None,
                 )
-    for part in range(n // group):
-        span = pl.ds(part * group * columns, group * columns)
-
-        def keep():
-            rsbuf[g, :, span] = outbuf[t, :, span]
+
+    plan = [(i, j, l) for i in range(nh) for l in range(2) for j in range(2)]
+    for i, j, l in plan[:2]:
+        produce(i, j, l)
+    for u in range(1, cuts[3]):
+        beside(3, *near, u)
+    for a in far:
+        beside(3, *a, 0)
+    for i, j, l in plan[2:6]:
+        produce(i, j, l)
+    for u in range(1, cuts[3]):
+        for a in far:
+            beside(3, *a, u)
+    for i, j, l in plan[6:]:
+        produce(i, j, l)
+    columns = obuf.shape[2]
+    for i, j, l in plan:
+        index = sp_of((zh + i) % nh, (zl + j) % 2, (y + l) % 2)
+
+        def keep(index=index):
+            rsbuf[g, index] = outbuf[index, pl.ds(pl.multiple_of(t * rows, rows), rows)]
 
         pl.when(own)(keep)
         total = None
         for r in range(nx):
-            for j in range(2):
-                index = tp_of((x + r) % nx, (zl + j) % 2)
+            for e in range(2):
+                other = tp_of((x + r) % nx, (zl + e) % 2)
                 receive(
-                    rsbuf.at[index, :, span], r_recv.at[part, index],
-                    apart if r == 0 and j == 0 else None,
+                    rsbuf.at[other, index], r_recv.at[index, other],
+                    apart if r == 0 and e == 0 else None,
                 )
-                term = rsbuf[index, :, span].astype(F32)
+                term = rsbuf[other, index].astype(F32)
                 total = term if total is None else total + term
+        span = pl.ds(pl.multiple_of(index * columns, columns), columns)
         out_ref[:, span] = total.astype(BF16)
-
     for copy, condition in started:
         guarded(condition, copy.wait_send)
 
@@ -602,7 +670,7 @@
     angles = np.arange(n * tok, dtype=np.float32)[:, None] * inverse[None, :]
     table = np.concatenate([np.cos(angles), np.sin(angles)], axis=1).astype(np.float32)
     wide_a = 2 * HEAD + heads * HEAD
-    wide_b = 3 * heads * HEAD
+    wide_b, wide_c = 2 * heads * HEAD, heads * HEAD
     deep = w_key_ret.shape[0]
     deep_o = w_out_ret.shape[0] + w_out_att.shape[0]
     tall = (heads // 2 + 1) * HEAD
@@ -622,33 +690,36 @@
             pltpu.VMEM((tok + rows, depth), BF16),
             pltpu.VMEM((n + 1, wide_a, deep), BF16),
             pltpu.VMEM((n + 1, wide_b, deep), BF16),
+            pltpu.VMEM((n + 1, wide_c, deep), BF16),
             pltpu.VMEM((n + 1, deep_o, w_out_ret.shape[1]), BF16),
             pltpu.VMEM((n, tok, 2 * HEAD), BF16),
             pltpu.VMEM((n, tall, 2 * HEAD), BF16),
             pltpu.VMEM((heads, HEAD, HEAD), F32),
-            pltpu.VMEM((heads, tok, HEAD), F32),
-            pltpu.VMEM((heads, tok, HEAD), F32),
-            pltpu.VMEM((m, rows, depth), BF16),
-            pltpu.VMEM((m, rows, depth), BF16),
+            pltpu.VMEM((heads * tok, 2 * HEAD), F32),
+            pltpu.VMEM((heads * tok, 2 * HEAD), BF16),
+            pltpu.VMEM((heads * tok, LANES), F32),
+            pltpu.VMEM((n, tok, w_out_ret.shape[1]), BF16),
+            pltpu.VMEM((m, n, rows, w_out_ret.shape[1]), BF16),
             dma((12,)),
             dma((2,)),
             dma((2,)),
             dma((1 + nx, TOKEN_CUT)),
             dma((nx - 1, 2, TOKEN_CUT)),
             dma((m, TOKEN_CUT)),
-            dma((3, nh, 2, CUT)),
-            dma((3, 2, CUT)),
-            dma((3, nh, 2, 2, CUT)),
-            dma((3, nh, 2, CUT)),
-            dma((3, n, 2, CUT)),
+            dma((len(CUTS), nh, 2, max(CUTS))),
+            dma((len(CUTS), 2, max(CUTS))),
+            dma((len(CUTS), nh, 2, 2, max(CUTS))),
+            dma((len(CUTS), nh, 2, max(CUTS))),
+            dma((len(CUTS), n, 2, max(CUTS))),
             dma((1, nh - 1)),
             dma((1, nh)),
             dma((1, nh, 2)),
             dma((1, n)),
             dma((nh, 2, 2)),
+            dma((nh, 2, 2)),
             dma((n,)),
-            dma((n // 2, nx, 2)),
-            dma((n // 2, m)),
+            dma((n, nx, 2)),
+            dma((n, m)),
         ],
         compiler_params=pltpu.CompilerParams(
             collective_id=0, has_side_effects=True, vmem_limit_bytes=60 * 1024 * 1024

time: 69.3 us -> 65 us (0.938)
  Pallas kernels: 67.4 us -> 63.1 us
    pallas_call x1, Pallas kernels: 67.4 us -> 63.1 us  [body(): pl.pallas_call(functools.partial(kernel, n, m, heads), out_shape=jax.Shap...]
where the time goes in v3:
time: 65 us; the launch traced here: 64.8 us
  Pallas kernels  63.1 us (97%)
  local copies, waits for them, and re-layouts  1.67 us (3%)
    pallas_call x1, Pallas kernels, body(): pl.pallas_call(functools.partial(kernel, n, m, heads), out_shape=jax.Shap...  63.1 us
    unnamed x1, local copies, waits for them, and re-layouts  1.67 us

profile of v3, /device:TPU:17, one launch (start us, length us, event | category | flops | bytes accessed | tf_op | source)
XLA Modules:
  0.0 64.8 jit_solution(2308087379995134770)
XLA Ops:
  0.0 63.1 %shard_map.127 = bf16[64,2048]{1,0:T(8,128)(2,1)} custom-call(bf16[64,2048]{1,0:T(8,128)(2,1)} %tok_hbm.1, f32[1,2048]{1,0:T(1,128)} %bitcast.14, bf16[192,256]{1,0:T(8,128)(2,1)} %bitcast.8, bf16[192,256]{1,0:T(8,128)(2,1)} %bitcast.9, bf16[192,256]{1,0:T(8,128)(2,1)} %bitcast.10, bf16[192,256]{1,0:T(8,128)(2,1)} %bitcast.11, bf16[64,256]{1,0:T(8,128)(2,1)} %bitcast.12, ...), custom_call_target="tpu_custom_call" | custom-call | tf_op jit(solution)/shard_map/pallas_call | solution.py:680
  63.2 1.7 %copy.15 = bf16[64,2048]{1,0:T(8,128)(2,1)} copy(bf16[64,2048]{1,0:T(8,128)(2,1)} %shard_map.127) | data formatting | bytes 524288

commit v4 on v3

--- a/solution.py
+++ b/solution.py
@@ -32,7 +32,7 @@
     m,
     heads,
     tok_hbm,
-    gain_ref,
+    gain_hbm,
     wq_ret_hbm,
     wk_ret_hbm,
     wv_ret_hbm,
@@ -62,24 +62,26 @@
     cbuf_gate,
     outbuf,
     rsbuf,
+    gain,
     load,
     small_send,
     small_recv,
     x_send,
     x_fwd,
-    x_recv,
-    w_send,
-    w_near,
+    x_pass,
+    x_other,
+    w_out,
     w_part,
-    w_y,
-    w_recv,
+    first_a,
+    first_b,
+    first_c,
+    first_o,
+    w_second,
+    o_second,
     k_send,
     k_y,
     k_part,
     k_recv,
-    st_send,
-    st_fwd,
-    st_recv,
     r_send,
     r_recv,
 ):
@@ -109,25 +111,32 @@
 
     slot = jnp.where(own, s, n)
     piece = jnp.where(own, t, m)
-    loads = [
-        pltpu.make_async_copy(source, target, load.at[k])
-        for k, (source, target) in enumerate((
-            (tok_hbm, tokens),
+    groups = (
+        (tokens, ((tok_hbm, tokens),)),
+        (gain, ((gain_hbm, gain),)),
+        (abuf.at[slot], (
             (wk_att_hbm, abuf.at[slot, pl.ds(0, HEAD)]),
             (wv_att_hbm, abuf.at[slot, pl.ds(HEAD, HEAD)]),
             (wq_att_hbm, abuf.at[slot, pl.ds(2 * HEAD, width)]),
+        )),
+        (bbuf.at[slot], (
             (wk_ret_hbm, bbuf.at[slot, pl.ds(0, width)]),
             (wv_ret_hbm, bbuf.at[slot, pl.ds(width, width)]),
-            (wq_ret_hbm, cbuf.at[slot]),
+        )),
+        (cbuf.at[slot], ((wq_ret_hbm, cbuf.at[slot]),)),
+        (obuf.at[slot], (
             (wo_ret_hbm, obuf.at[slot, pl.ds(0, half_o)]),
             (wo_att_hbm, obuf.at[slot, pl.ds(half_o, wo_att_hbm.shape[0])]),
-            (table_hbm.at[pl.ds(pl.multiple_of(q * tok, tok), tok)], table),
-            (logs_hbm, lbuf.at[0]),
-            (gate_hbm, gbuf.at[0]),
-        ))
-    ]
-    for copy in loads:
-        copy.start()
+        )),
+        (table, ((table_hbm.at[pl.ds(pl.multiple_of(q * tok, tok), tok)], table),)),
+        (lbuf.at[0], ((logs_hbm, lbuf.at[0]),)),
+        (gbuf.at[0], ((gate_hbm, gbuf.at[0]),)),
+    )
+    loads = []
+    for k, (whole, copies) in enumerate(groups):
+        for source, target in copies:
+            pltpu.make_async_copy(source, target, load.at[k]).start()
+        loads.append(pltpu.make_async_copy(whole, whole, load.at[k]))
 
     barrier = pltpu.get_barrier_semaphore()
     greeted = [
@@ -153,13 +162,23 @@
         else:
             pl.when(condition)(action)
 
-    def send(source, target, send_sem, recv_sem, where, condition=None):
+    def send(source, target, send_sem, recv_sem, where, condition=None, kept=True):
         copy = pltpu.make_async_remote_copy(
             src_ref=source, dst_ref=target, send_sem=send_sem, recv_sem=recv_sem,
             device_id=where, device_id_type=MESH,
         )
         guarded(condition, copy.start)
-        started.append((copy, condition))
+        if kept:
+            started.append((copy, condition))
+
+    def drain(source, send_sem, condition=None):
+        started.append((
+            pltpu.make_async_remote_copy(
+                src_ref=source, dst_ref=source, send_sem=send_sem, recv_sem=send_sem,
+                device_id=partner, device_id_type=MESH,
+            ),
+            condition,
+        ))
 
     def receive(target, recv_sem, condition=None):
         copy = pltpu.make_async_remote_copy(
@@ -168,13 +187,14 @@
         )
         guarded(condition, copy.wait_recv)
 
-    loads[0].wait()
+    for copy in loads[:2]:
+        copy.wait()
     values = tokens[...].astype(F32)
     scale = lax.rsqrt(jnp.mean(values * values, axis=-1, keepdims=True) + EPS)
     xbuf[pl.ds(pl.multiple_of(piece * rows, rows), rows), :] = (
-        values * scale * gain_ref[...]
+        values * scale * gain[...]
     ).astype(BF16)
-    for copy in loads[1:]:
+    for copy in loads[2:]:
         copy.wait()
     pl.semaphore_wait(barrier, len(greeted))
 
@@ -186,12 +206,19 @@
         start = pl.multiple_of((k * cuts[p] + u) * length, length)
         return parts[p].at[index, pl.ds(start, length)]
 
+    firsts = (first_a, first_b, first_c, first_o)
+
+    def second(p, index):
+        return o_second.at[index] if p == 3 else w_second.at[p]
+
+    def halves(p, count):
+        return parts[p].at[pl.ds(0, count), pl.ds(0, parts[p].shape[1] // 2)]
+
     def scatter_one(p, i, k, u, condition):
         core = (c + k) % 2
         send(
-            chunk(p, slot, core, u), chunk(p, s, core, u),
-            w_send.at[p, i, k, u], w_recv.at[p, s, core, u],
-            device((zh + i) % nh, c, y, x, core), condition,
+            chunk(p, slot, core, u), chunk(p, s, core, u), w_out.at[p], firsts[p].at[s, u],
+            device((zh + i) % nh, c, y, x, core), condition, False,
         )
 
     def scatter_chip(p):
@@ -200,12 +227,7 @@
 
     def scatter_near(p, u):
         for k in range(2):
-            core = (c + k) % 2
-            send(
-                chunk(p, slot, core, u), chunk(p, s, core, u),
-                w_near.at[p, k, u], w_recv.at[p, s, core, u],
-                device(zh, c, y, x, core), apart,
-            )
+            scatter_one(p, 0, k, u, apart)
 
     def scatter_far(p, u, condition=None):
         for i in range(1, nh):
@@ -219,49 +241,39 @@
         index = sp_of((zh + i) % nh, (zl + j) % 2, y)
         here = i == 0 and j == 0
         spot = chunk(p, index, c, u)
-        receive(spot, w_recv.at[p, index, c, u], apart if here else condition)
-        send(spot, spot, w_y.at[p, i, j, u], w_recv.at[p, index, c, u], across, condition)
+        receive(spot, firsts[p].at[index, u], apart if here else condition)
+        send(spot, spot, w_out.at[p], firsts[p].at[index, u], across, condition, False)
         send(
-            spot, spot, w_part.at[p, i, j, 0, u], w_recv.at[p, index, c, u], partner,
-            own if here else condition,
+            spot, spot, w_part.at[p], second(p, index), partner,
+            own if here else condition, False,
         )
 
     def beside(p, i, j, u):
         index = sp_of((zh + i) % nh, (zl + j) % 2, 1 - y)
         spot = chunk(p, index, c, u)
-        receive(spot, w_recv.at[p, index, c, u])
-        send(spot, spot, w_part.at[p, i, j, 1, u], w_recv.at[p, index, c, u], partner)
-
-    def ready(p, i, j, l):
-        index = sp_of((zh + i) % nh, (zl + j) % 2, (y + l) % 2)
-        for u in range(cuts[p]):
-            receive(
-                chunk(p, index, 1 - c, u), w_recv.at[p, index, 1 - c, u],
-                apart if i == 0 and j == 0 and l == 0 else None,
-            )
+        receive(spot, firsts[p].at[index, u])
+        send(spot, spot, w_part.at[p], second(p, index), partner, None, False)
 
     def rest(p):
-        for i in range(nh):
-            for j in range(2):
-                for l in range(2):
-                    ready(p, i, j, l)
+        receive(halves(p, n - 1), w_second.at[p], own)
+        receive(halves(p, n), w_second.at[p], apart)
 
     far = [(i, j) for i in range(1, nh) for j in range(2)]
     near = (0, 1)
-    pieces = x_recv.shape[1]
+    pieces = x_pass.shape[1]
 
     def rows_of(index, u):
         length = rows // pieces
         return xbuf.at[pl.ds(pl.multiple_of((index * pieces + u) * length, length), length)]
 
     def pass_tokens(k, u):
-        index = tp_of(x, (c + k) % 2)
+        core = (c + k) % 2
+        index = tp_of(x, core)
         spot = rows_of(index, u)
-        receive(spot, x_recv.at[index, u], apart if k == 0 else None)
+        receive(spot, x_pass.at[core, u], apart if k == 0 else None)
         for r in range(1, nx):
             send(
-                spot, spot, x_fwd.at[r - 1, k, u], x_recv.at[index, u],
-                device(zh, zl, y, (x + r) % nx, c), apart,
+                spot, spot, x_fwd, x_other, device(zh, zl, y, (x + r) % nx, c), apart, False,
             )
 
     send(
@@ -273,19 +285,13 @@
         scatter_far(0, u)
     scatter_chip(0)
     for u in range(pieces):
-        send(
-            rows_of(piece, u), rows_of(t, u), x_send.at[0, u], x_recv.at[t, u],
-            device(zh, 1 - zl, y, x, zl),
-        )
+        ours, there = rows_of(piece, u), rows_of(t, u)
+        send(ours, there, x_send, x_pass.at[c, u], device(zh, 1 - zl, y, x, zl), None, False)
         for r in range(1, nx):
             send(
-                rows_of(piece, u), rows_of(t, u), x_send.at[1 + r, u], x_recv.at[t, u],
-                device(zh, zl, y, (x + r) % nx, zl),
+                ours, there, x_send, x_other, device(zh, zl, y, (x + r) % nx, zl), None, False,
             )
-        send(
-            rows_of(piece, u), rows_of(t, u), x_send.at[1, u], x_recv.at[t, u],
-            device(zh, zl, y, x, zl), apart,
-        )
+        send(ours, there, x_send, x_pass.at[c, u], device(zh, zl, y, x, zl), apart, False)
     for u in range(cuts[0]):
         scatter_near(0, u)
     for p in range(1, 4):
@@ -348,11 +354,7 @@
     for a in far:
         entry(1, *a, 0, outer)
 
-    for r in range(1, nx):
-        for k in range(2):
-            index = tp_of((x + r) % nx, k)
-            for u in range(pieces):
-                receive(rows_of(index, u), x_recv.at[index, u])
+    receive(xbuf.at[pl.ds(0, (m - 2) * rows)], x_other)
     rest(0)
 
     def exchange(buf, e, index, sem, where, condition):
@@ -504,19 +506,7 @@
         spot = slice(k % 2 * HEAD, (k % 2 + 1) * HEAD)
         return stbuf[index, k // 2 * HEAD : (k // 2 + 1) * HEAD, spot].astype(F32)
 
-    for i in range(1, nh):
-        send(
-            stbuf.at[q], stbuf.at[q], st_send.at[i, 0, 0], st_recv.at[q],
-            device((zh + i) % nh, zl, y, x, c), zh + i < nh,
-        )
-    for l in range(2):
-        for e in range(2):
-            if l or e:
-                index = sp_of(zh, (c + e) % 2, (y + l) % 2)
-                send(
-                    stbuf.at[q], stbuf.at[q], st_send.at[0, l, e], st_recv.at[q],
-                    device(zh, zl, (y + l) % 2, x, (c + e) % 2), index > q,
-                )
+    exchange_send(stbuf, 1)
     for u in range(1, cuts[3]):
         scatter_far(3, u, zh < nh - 1)
     for u in range(cuts[2]):
@@ -526,16 +516,7 @@
     entry(3, *near, 0)
     rest(2)
 
-    for i in range(1, nh):
-        index = sp_of((zh + nh - i) % nh, c, y)
-        receive(stbuf.at[index], st_recv.at[index], zh >= i)
-        for l in range(2):
-            for e in range(2):
-                if l or e:
-                    send(
-                        stbuf.at[index], stbuf.at[index], st_fwd.at[i, l, e], st_recv.at[index],
-                        device(zh, zl, (y + l) % 2, x, (c + e) % 2), zh >= i,
-                    )
+    exchange_far(stbuf, 1)
     proj = project(cbuf)
     local, lifts = [], []
     for h in range(heads):
@@ -547,6 +528,7 @@
         local.append(dot(weights, vals[h]))
         lifts.append((query.astype(F32) * jnp.exp(column)).astype(BF16))
     exchange_far_part(kvbuf, 0)
+    exchange_across(stbuf, 1)
     steps = [(beside, near, 0)]
     steps += [(entry, a, u) for u in range(1, cuts[3]) for a in far]
     steps += [(entry, near, u) for u in range(1, cuts[3])]
@@ -561,17 +543,9 @@
             steps = steps[1:]
     for call, a, u in steps:
         call(3, *a, u)
-    for i in range(1, nh):
-        for l in range(2):
-            for e in range(2):
-                if l or e:
-                    index = sp_of((zh + nh - i) % nh, (c + e) % 2, (y + l) % 2)
-                    receive(stbuf.at[index], st_recv.at[index], zh >= i)
-    for l in range(2):
-        for e in range(2):
-            if l or e:
-                index = sp_of(zh, (c + e) % 2, (y + l) % 2)
-                receive(stbuf.at[index], st_recv.at[index], index < q)
+    exchange_far_across(stbuf, 1)
+    exchange_part(stbuf, 1)
+    exchange_far_part(stbuf, 1)
     state[...] = jnp.zeros_like(state)
     for j in range(n - 1):
         def earlier(j=j):
@@ -594,53 +568,55 @@
 
     def produce(i, j, l):
         index = sp_of((zh + i) % nh, (zl + j) % 2, (y + l) % 2)
-        ready(3, i, j, l)
+        receive(
+            halves(3, 1), o_second.at[index], apart if i == 0 and j == 0 and l == 0 else None
+        )
         outbuf[index] = dot(mixed, obuf[index]).astype(BF16)
         for r in reversed(range(nx)):
             for k in range(2):
                 where = tp_of((x + r) % nx, (c + k) % 2)
                 rows_there = pl.ds(pl.multiple_of(where * rows, rows), rows)
                 send(
-                    outbuf.at[index, rows_there], rsbuf.at[g, index],
-                    r_send.at[index, r, k], r_recv.at[index, g],
+                    outbuf.at[index, rows_there], rsbuf.at[index, g], r_send, r_recv.at[index],
                     device(zh, c, y, (x + r) % nx, (c + k) % 2),
-                    apart if r == 0 and k == 0 else None,
+                    apart if r == 0 and k == 0 else None, False,
                 )
 
-    plan = [(i, j, l) for i in range(nh) for l in range(2) for j in range(2)]
-    for i, j, l in plan[:2]:
-        produce(i, j, l)
+    for i, j in order:
+        produce(i, j, 0)
     for u in range(1, cuts[3]):
         beside(3, *near, u)
-    for a in far:
-        beside(3, *a, 0)
-    for i, j, l in plan[2:6]:
-        produce(i, j, l)
-    for u in range(1, cuts[3]):
+    for u in range(cuts[3]):
         for a in far:
             beside(3, *a, u)
-    for i, j, l in plan[6:]:
-        produce(i, j, l)
+    for i, j in order:
+        produce(i, j, 1)
     columns = obuf.shape[2]
-    for i, j, l in plan:
-        index = sp_of((zh + i) % nh, (zl + j) % 2, (y + l) % 2)
-
-        def keep(index=index):
-            rsbuf[g, index] = outbuf[index, pl.ds(pl.multiple_of(t * rows, rows), rows)]
-
-        pl.when(own)(keep)
-        total = None
-        for r in range(nx):
-            for e in range(2):
-                other = tp_of((x + r) % nx, (zl + e) % 2)
-                receive(
-                    rsbuf.at[other, index], r_recv.at[index, other],
-                    apart if r == 0 and e == 0 else None,
-                )
-                term = rsbuf[other, index].astype(F32)
-                total = term if total is None else total + term
-        span = pl.ds(pl.multiple_of(index * columns, columns), columns)
-        out_ref[:, span] = total.astype(BF16)
+    for l in range(2):
+        for i, j in order:
+            index = sp_of((zh + i) % nh, (zl + j) % 2, (y + l) % 2)
+
+            def keep(index=index):
+                rsbuf[index, g] = outbuf[index, pl.ds(pl.multiple_of(t * rows, rows), rows)]
+
+            receive(rsbuf.at[index, pl.ds(0, m - 1)], r_recv.at[index], own)
+            pl.when(own)(keep)
+            receive(rsbuf.at[index], r_recv.at[index], apart)
+            total = rsbuf[index, 0].astype(F32)
+            for other in range(1, m):
+                total = total + rsbuf[index, other].astype(F32)
+            span = pl.ds(pl.multiple_of(index * columns, columns), columns)
+            out_ref[:, span] = total.astype(BF16)
+    for p in range(4):
+        drain(halves(p, n - 1), w_out.at[p], own)
+        drain(halves(p, n), w_out.at[p], apart)
+        drain(halves(p, n), w_part.at[p], own)
+        drain(halves(p, n - 1), w_part.at[p], apart)
+    drain(xbuf.at[pl.ds(0, nx * rows)], x_send, own)
+    drain(xbuf.at[pl.ds(0, (nx + 1) * rows)], x_send, apart)
+    drain(xbuf.at[pl.ds(0, (m - 2) * rows)], x_fwd, apart)
+    drain(rsbuf.at[:, pl.ds(0, m - 1)], r_send, own)
+    drain(rsbuf, r_send, apart)
     for copy, condition in started:
         guarded(condition, copy.wait_send)
 
@@ -680,7 +656,7 @@
     return pl.pallas_call(
         functools.partial(kernel, n, m, heads),
         out_shape=jax.ShapeDtypeStruct((rows, depth), BF16),
-        in_specs=[hbm, vmem] + [hbm] * 11,
+        in_specs=[hbm] * 13,
         out_specs=vmem,
         scratch_shapes=[
             pltpu.VMEM(tokens.shape, BF16),
@@ -699,27 +675,26 @@
             pltpu.VMEM((heads * tok, 2 * HEAD), BF16),
             pltpu.VMEM((heads * tok, LANES), F32),
             pltpu.VMEM((n, tok, w_out_ret.shape[1]), BF16),
-            pltpu.VMEM((m, n, rows, w_out_ret.shape[1]), BF16),
-            dma((12,)),
+            pltpu.VMEM((n, m, rows, w_out_ret.shape[1]), BF16),
+            pltpu.VMEM((1, depth), F32),
+            dma((9,)),
             dma((2,)),
             dma((2,)),
-            dma((1 + nx, TOKEN_CUT)),
-            dma((nx - 1, 2, TOKEN_CUT)),
-            dma((m, TOKEN_CUT)),
-            dma((len(CUTS), nh, 2, max(CUTS))),
-            dma((len(CUTS), 2, max(CUTS))),
-            dma((len(CUTS), nh, 2, 2, max(CUTS))),
-            dma((len(CUTS), nh, 2, max(CUTS))),
-            dma((len(CUTS), n, 2, max(CUTS))),
-            dma((1, nh - 1)),
-            dma((1, nh)),
-            dma((1, nh, 2)),
-            dma((1, n)),
-            dma((nh, 2, 2)),
-            dma((nh, 2, 2)),
+            dma,
+            dma,
+            dma((2, TOKEN_CUT)),
+            dma,
+            dma((len(CUTS),)),
+            dma((len(CUTS),)),
+            *[dma((n, count)) for count in CUTS],
+            dma((len(CUTS) - 1,)),
             dma((n,)),
-            dma((n, nx, 2)),
-            dma((n, m)),
+            dma((2, nh - 1)),
+            dma((2, nh)),
+            dma((2, nh, 2)),
+            dma((2, n)),
+            dma,
+            dma((n,)),
         ],
         compiler_params=pltpu.CompilerParams(
             collective_id=0, has_side_effects=True, vmem_limit_bytes=60 * 1024 * 1024

time: 65 us -> 61.5 us (0.946)
  Pallas kernels: 63.1 us -> 59.6 us
    pallas_call x1, Pallas kernels: 63.1 us -> 59.6 us  [body(): pl.pallas_call(functools.partial(kernel, n, m, heads), out_shape=jax.Shap...]
where the time goes in v4:
time: 61.5 us; the launch traced here: 61.3 us
  Pallas kernels  59.6 us (97%)
  local copies, waits for them, and re-layouts  1.67 us (3%)
    pallas_call x1, Pallas kernels, body(): pl.pallas_call(functools.partial(kernel, n, m, heads), out_shape=jax.Shap...  59.6 us
    unnamed x1, local copies, waits for them, and re-layouts  1.67 us

profile of v4, /device:TPU:17, one launch (start us, length us, event | category | flops | bytes accessed | tf_op | source)
XLA Modules:
  0.0 61.3 jit_solution(4021565088843491039)
XLA Ops:
  0.0 59.6 %shard_map.127 = bf16[64,2048]{1,0:T(8,128)(2,1)} custom-call(bf16[64,2048]{1,0:T(8,128)(2,1)} %tok_hbm.1, f32[1,2048]{1,0:T(1,128)} %bitcast.14, bf16[192,256]{1,0:T(8,128)(2,1)} %bitcast.8, bf16[192,256]{1,0:T(8,128)(2,1)} %bitcast.9, bf16[192,256]{1,0:T(8,128)(2,1)} %bitcast.10, bf16[192,256]{1,0:T(8,128)(2,1)} %bitcast.11, bf16[64,256]{1,0:T(8,128)(2,1)} %bitcast.12, ...), custom_call_target="tpu_custom_call" | custom-call | tf_op jit(solution)/shard_map/pallas_call | solution.py:656
  59.7 1.7 %copy.15 = bf16[64,2048]{1,0:T(8,128)(2,1)} copy(bf16[64,2048]{1,0:T(8,128)(2,1)} %shard_map.127) | data formatting | bytes 524288

commit v5 on v4

--- a/solution.py
+++ b/solution.py
@@ -17,9 +17,9 @@
 SPAN = 256
 KEY_SPAN = 256
 LANES = 128
-CUTS = (2, 2, 1, 2)
+CUTS = (2, 2, 1, 3)
 LOG2E = float(np.log2(np.e))
-TOKEN_CUT = 2
+TOKEN_CUT = 4
 HIGH = lax.Precision.HIGHEST
 
 
@@ -284,7 +284,7 @@
     for u in range(cuts[0]):
         scatter_far(0, u)
     scatter_chip(0)
-    for u in range(pieces):
+    def give_tokens(u):
         ours, there = rows_of(piece, u), rows_of(t, u)
         send(ours, there, x_send, x_pass.at[c, u], device(zh, 1 - zl, y, x, zl), None, False)
         for r in range(1, nx):
@@ -292,8 +292,13 @@
                 ours, there, x_send, x_other, device(zh, zl, y, (x + r) % nx, zl), None, False,
             )
         send(ours, there, x_send, x_pass.at[c, u], device(zh, zl, y, x, zl), apart, False)
+
+    for u in range(pieces // 2):
+        give_tokens(u)
     for u in range(cuts[0]):
         scatter_near(0, u)
+    for u in range(pieces // 2, pieces):
+        give_tokens(u)
     for p in range(1, 4):
         scatter_chip(p)
     for p in range(1, 3):
@@ -327,8 +332,9 @@
         beside(0, 0, 0, u)
     for a in far:
         entry(0, *a, 0)
-    for k in range(2):
-        pass_tokens(k, 0)
+    for u in range(pieces // 2):
+        for k in range(2):
+            pass_tokens(k, u)
     for u in range(cuts[1]):
         beside(1, 0, 0, u)
     for u in range(1, cuts[0]):
@@ -336,11 +342,11 @@
             entry(0, *a, u)
     for a in far:
         beside(0, *a, 0)
-    for u in range(1, pieces):
+    for u in range(cuts[0]):
+        entry(0, *near, u)
+    for u in range(pieces // 2, pieces):
         for k in range(2):
             pass_tokens(k, u)
-    for u in range(cuts[0]):
-        entry(0, *near, u)
     for a in far:
         entry(1, *a, 0, middle)
     for u in range(1, cuts[0]):
@@ -351,6 +357,9 @@
             beside(p, 0, 0, u)
     for u in range(cuts[0]):
         beside(0, *near, u)
+    for u in range(1, cuts[1]):
+        for a in far:
+            entry(1, *a, u, middle)
     for a in far:
         entry(1, *a, 0, outer)
 
@@ -415,9 +424,6 @@
     exchange_send(kvbuf, 0)
     scatter_far(3, 0)
     scatter_near(3, 0)
-    for u in range(1, cuts[3]):
-        scatter_far(3, u, zh == nh - 1)
-        scatter_near(3, u)
     wide = heads * tok
     zeros = jnp.zeros((tok, HEAD), F32)
     for h in range(heads):
@@ -450,7 +456,7 @@
 
     for u in range(1, cuts[1]):
         for a in far:
-            entry(1, *a, u)
+            entry(1, *a, u, outer)
     attend([q], True)
     for a in far:
         beside(1, *a, 0)
@@ -460,7 +466,6 @@
     exchange_part(kvbuf, 0)
     index = sp_of(zh, 0, 0)
     pl.when(index < q)(functools.partial(attend, [index]))
-    exchange_far(kvbuf, 0)
     pl.when(index + 1 < q)(functools.partial(attend, [index + 1]))
     for u in range(1, cuts[1]):
         for a in far:
@@ -473,11 +478,8 @@
         beside(1, *near, u)
     for u in range(cuts[2]):
         entry(2, *near, u)
-    exchange_far_across(kvbuf, 0)
-    for a in far:
-        entry(3, *a, 0)
+    exchange_far(kvbuf, 0)
     rest(1)
-
     proj = project(bbuf)
     keys, vals, updates, marks = [], [], [], []
     for h in range(heads):
@@ -508,15 +510,18 @@
 
     exchange_send(stbuf, 1)
     for u in range(1, cuts[3]):
-        scatter_far(3, u, zh < nh - 1)
+        scatter_far(3, u)
+        scatter_near(3, u)
+    for a in far:
+        entry(3, *a, 0)
     for u in range(cuts[2]):
         for a in far:
             beside(2, *a, u)
         beside(2, *near, u)
+    exchange_far(stbuf, 1)
     entry(3, *near, 0)
     rest(2)
 
-    exchange_far(stbuf, 1)
     proj = project(cbuf)
     local, lifts = [], []
     for h in range(heads):
@@ -527,23 +532,22 @@
         weights = jnp.where(causal, scores * jnp.exp(gap), 0.0).astype(BF16)
         local.append(dot(weights, vals[h]))
         lifts.append((query.astype(F32) * jnp.exp(column)).astype(BF16))
+    exchange_far_across(kvbuf, 0)
     exchange_far_part(kvbuf, 0)
+
+    def attend_far(half):
+        for i in range(1, nh):
+            index = sp_of((zh + nh - i) % nh, 0, 0) + 2 * half
+            pl.when(zh >= i)(functools.partial(attend, [index, index + 1]))
+
+    attend_far(0)
     exchange_across(stbuf, 1)
-    steps = [(beside, near, 0)]
-    steps += [(entry, a, u) for u in range(1, cuts[3]) for a in far]
-    steps += [(entry, near, u) for u in range(1, cuts[3])]
-    for i in range(1, nh):
-        index = sp_of((zh + nh - i) % nh, 0, 0)
-        for half in range(2):
-            pl.when(zh >= i)(
-                functools.partial(attend, [index + 2 * half, index + 2 * half + 1])
-            )
-            for call, a, u in steps[:1]:
-                call(3, *a, u)
-            steps = steps[1:]
-    for call, a, u in steps:
-        call(3, *a, u)
     exchange_far_across(stbuf, 1)
+    attend_far(1)
+    for u in range(1, cuts[3]):
+        for a in far:
+            entry(3, *a, u)
+        entry(3, *near, u)
     exchange_part(stbuf, 1)
     exchange_far_part(stbuf, 1)
     state[...] = jnp.zeros_like(state)
@@ -584,7 +588,7 @@
 
     for i, j in order:
         produce(i, j, 0)
-    for u in range(1, cuts[3]):
+    for u in range(cuts[3]):
         beside(3, *near, u)
     for u in range(cuts[3]):
         for a in far:

time: 61.5 us -> 59.9 us (0.974)
  Pallas kernels: 59.6 us -> 58.1 us
    pallas_call x1, Pallas kernels: 59.6 us -> 58.1 us  [body(): pl.pallas_call(functools.partial(kernel, n, m, heads), out_shape=jax.Shap...]
where the time goes in v5:
time: 59.9 us; the launch traced here: 59.8 us
  Pallas kernels  58.1 us (97%)
  local copies, waits for them, and re-layouts  1.67 us (3%)
    pallas_call x1, Pallas kernels, body(): pl.pallas_call(functools.partial(kernel, n, m, heads), out_shape=jax.Shap...  58.1 us
    unnamed x1, local copies, waits for them, and re-layouts  1.67 us

profile of v5, /device:TPU:17, one launch (start us, length us, event | category | flops | bytes accessed | tf_op | source)
XLA Modules:
  0.0 59.8 jit_solution(658000872727165011)
XLA Ops:
  0.0 58.1 %shard_map.127 = bf16[64,2048]{1,0:T(8,128)(2,1)} custom-call(bf16[64,2048]{1,0:T(8,128)(2,1)} %tok_hbm.1, f32[1,2048]{1,0:T(1,128)} %bitcast.14, bf16[192,256]{1,0:T(8,128)(2,1)} %bitcast.8, bf16[192,256]{1,0:T(8,128)(2,1)} %bitcast.9, bf16[192,256]{1,0:T(8,128)(2,1)} %bitcast.10, bf16[192,256]{1,0:T(8,128)(2,1)} %bitcast.11, bf16[64,256]{1,0:T(8,128)(2,1)} %bitcast.12, ...), custom_call_target="tpu_custom_call" | custom-call | tf_op jit(solution)/shard_map/pallas_call | solution.py:660
  58.1 1.7 %copy.15 = bf16[64,2048]{1,0:T(8,128)(2,1)} copy(bf16[64,2048]{1,0:T(8,128)(2,1)} %shard_map.127) | data formatting | bytes 524288

commit v6 on v5

--- a/solution.py
+++ b/solution.py
@@ -56,12 +56,13 @@
     obuf,
     kvbuf,
     stbuf,
-    state,
+    decay,
     num,
     qbuf,
     cbuf_gate,
     outbuf,
     rsbuf,
+    passed,
     gain,
     load,
     small_send,
@@ -83,6 +84,7 @@
     k_part,
     k_recv,
     r_send,
+    r_pass,
     r_recv,
 ):
     s, t = lax.axis_index("sp"), lax.axis_index("tp")
@@ -138,6 +140,7 @@
             pltpu.make_async_copy(source, target, load.at[k]).start()
         loads.append(pltpu.make_async_copy(whole, whole, load.at[k]))
 
+    stbuf[...] = jnp.zeros_like(stbuf)
     barrier = pltpu.get_barrier_semaphore()
     greeted = [
         device((zh + i) % nh, zl, 1 - y, x, (c + k) % 2) for i in range(nh) for k in range(2)
@@ -327,6 +330,9 @@
         [gates_own, jnp.zeros((LANES - heads, tok), F32)], axis=0
     ).T
     cosine, sine = table[:, : HEAD // 2], table[:, HEAD // 2 :]
+    for h in range(heads):
+        gap = jnp.where(causal, within[:, h : h + 1] - turned[h : h + 1, :], 0.0)
+        decay[h] = jnp.where(causal, jnp.exp(gap), 0.0)
 
     for u in range(cuts[0]):
         beside(0, 0, 0, u)
@@ -389,12 +395,13 @@
         for k in range(2):
             arrive(buf, e, sp_of(zh, 1 - c, (y + k) % 2), c == 1)
 
-    def exchange_far(buf, e):
+    def exchange_far(buf, e, also=True):
         for i in range(1, nh):
             index = sp_of((zh + nh - i) % nh, c, y)
-            arrive(buf, e, index, zh >= i)
-            exchange(buf, e, index, k_y.at[e, i], across, zh >= i)
-            exchange(buf, e, index, k_part.at[e, i, 0], partner, zh >= i)
+            condition = (zh >= i) & also
+            arrive(buf, e, index, condition)
+            exchange(buf, e, index, k_y.at[e, i], across, condition)
+            exchange(buf, e, index, k_part.at[e, i, 0], partner, condition)
 
     def exchange_far_across(buf, e):
         for i in range(1, nh):
@@ -424,6 +431,8 @@
     exchange_send(kvbuf, 0)
     scatter_far(3, 0)
     scatter_near(3, 0)
+    for u in range(1, cuts[3]):
+        scatter_far(3, u, zh == nh - 1)
     wide = heads * tok
     zeros = jnp.zeros((tok, HEAD), F32)
     for h in range(heads):
@@ -510,7 +519,7 @@
 
     exchange_send(stbuf, 1)
     for u in range(1, cuts[3]):
-        scatter_far(3, u)
+        scatter_far(3, u, zh < nh - 1)
         scatter_near(3, u)
     for a in far:
         entry(3, *a, 0)
@@ -518,7 +527,8 @@
         for a in far:
             beside(2, *a, u)
         beside(2, *near, u)
-    exchange_far(stbuf, 1)
+    exchange_far_across(kvbuf, 0)
+    exchange_far(stbuf, 1, zl <= c)
     entry(3, *near, 0)
     rest(2)
 
@@ -527,12 +537,11 @@
     for h in range(heads):
         query = (rope(proj[:, h * HEAD : (h + 1) * HEAD]) * HEAD ** (-0.5)).astype(BF16)
         column = within[:, h : h + 1]
-        gap = jnp.where(causal, column - turned[h : h + 1, :], 0.0)
         scores = dot(query, keys[h], ((1,), (1,)))
-        weights = jnp.where(causal, scores * jnp.exp(gap), 0.0).astype(BF16)
+        weights = (scores * decay[h]).astype(BF16)
         local.append(dot(weights, vals[h]))
         lifts.append((query.astype(F32) * jnp.exp(column)).astype(BF16))
-    exchange_far_across(kvbuf, 0)
+    exchange_far(stbuf, 1, zl > c)
     exchange_far_part(kvbuf, 0)
 
     def attend_far(half):
@@ -540,28 +549,26 @@
             index = sp_of((zh + nh - i) % nh, 0, 0) + 2 * half
             pl.when(zh >= i)(functools.partial(attend, [index, index + 1]))
 
+    exchange_across(stbuf, 1)
     attend_far(0)
-    exchange_across(stbuf, 1)
+    attend_far(1)
     exchange_far_across(stbuf, 1)
-    attend_far(1)
     for u in range(1, cuts[3]):
         for a in far:
             entry(3, *a, u)
         entry(3, *near, u)
     exchange_part(stbuf, 1)
     exchange_far_part(stbuf, 1)
-    state[...] = jnp.zeros_like(state)
+    states = [jnp.zeros((HEAD, HEAD), F32)] * heads
     for j in range(n - 1):
-        def earlier(j=j):
-            marked = piece_of(j, heads)
-            for h in range(heads):
-                total = marked[16 * h : 16 * h + 1] + marked[16 * h + 8 : 16 * h + 9]
-                state[h] = jnp.exp(total) * state[h] + piece_of(j, h)
-
-        pl.when(q > j)(earlier)
+        marked = piece_of(j, heads)
+        for h in range(heads):
+            total = marked[16 * h : 16 * h + 1] + marked[16 * h + 8 : 16 * h + 9]
+            moved = jnp.exp(total) * states[h] + piece_of(j, h)
+            states[h] = jnp.where(q > j, moved, states[h])
     retained, attended = [], []
     for h in range(heads):
-        raw = local[h] + dot(lifts[h], state[h].astype(BF16))
+        raw = local[h] + dot(lifts[h], states[h].astype(BF16))
         centre = jnp.mean(raw, axis=-1, keepdims=True)
         spread = jnp.mean(jnp.square(raw - centre), axis=-1, keepdims=True)
         retained.append(((raw - centre) * lax.rsqrt(spread + EPS)).astype(BF16))
@@ -570,44 +577,113 @@
     mixed = jnp.concatenate(retained + attended, axis=-1)
     order = [(i, j) for i in range(nh) for j in range(2)]
 
-    def produce(i, j, l):
-        index = sp_of((zh + i) % nh, (zl + j) % 2, (y + l) % 2)
+    pair = 2 * rows
+    pair_here = pl.ds(pl.multiple_of(x * pair, pair), pair)
+
+    def slice_of(i, j, l):
+        return sp_of((zh + i) % nh, (zl + j) % 2, (y + l) % 2)
+
+    def multiply(i, j, l):
+        index = slice_of(i, j, l)
         receive(
             halves(3, 1), o_second.at[index], apart if i == 0 and j == 0 and l == 0 else None
         )
         outbuf[index] = dot(mixed, obuf[index]).astype(BF16)
+        return index
+
+    def give(index, spot, x_, c_, condition):
+        where = tp_of(x_, c_)
+        rows_there = pl.ds(pl.multiple_of(where * rows, rows), rows)
+        send(
+            outbuf.at[index, rows_there], rsbuf.at[index, spot], r_send, r_recv.at[index],
+            device(zh, c, y, x_, c_), condition, False,
+        )
+
+    def produce(i, j, l):
+        index = multiply(i, j, l)
         for r in reversed(range(nx)):
             for k in range(2):
-                where = tp_of((x + r) % nx, (c + k) % 2)
-                rows_there = pl.ds(pl.multiple_of(where * rows, rows), rows)
+                give(
+                    index, g, (x + r) % nx, (c + k) % 2, apart if r == 0 and k == 0 else None
+                )
+
+    def start_pair(i, j):
+        index = multiply(i, j, 0)
+        if i % 2:
+            send(
+                outbuf.at[index], passed.at[index], r_send, r_pass.at[index],
+                device(zh, 1 - zl, y, x, c), apart, False,
+            )
+        else:
+            for r in range(1, nx):
+                other = (x + r) % nx
                 send(
-                    outbuf.at[index, rows_there], rsbuf.at[index, g], r_send, r_recv.at[index],
-                    device(zh, c, y, (x + r) % nx, (c + k) % 2),
-                    apart if r == 0 and k == 0 else None, False,
+                    outbuf.at[index, pl.ds(pl.multiple_of(other * pair, pair), pair)],
+                    passed.at[index, pl.ds((r - 1) * pair, pair)], r_send, r_pass.at[index],
+                    device(zh, zl, y, other, c), None, False,
                 )
 
+    def finish_pair(i, j):
+        index = slice_of(i, j, 0)
+        if i % 2:
+            receive(passed.at[index], r_pass.at[index], own)
+
+            def merge():
+                outbuf[index] = (
+                    outbuf[index].astype(F32) + passed[index].astype(F32)
+                ).astype(BF16)
+
+            pl.when(own)(merge)
+            for r in reversed(range(nx)):
+                for k in range(2):
+                    if r or k:
+                        give(index, x, (x + r) % nx, (c + k) % 2, own)
+        else:
+            receive(passed.at[index, pl.ds(0, (nx - 1) * pair)], r_pass.at[index])
+            total = outbuf[index, pair_here].astype(F32)
+            for r in range(1, nx):
+                total = total + passed[index, (r - 1) * pair : r * pair].astype(F32)
+            outbuf[index, pair_here] = total.astype(BF16)
+            for k in (1, 0):
+                give(index, zl, x, (c + k) % 2, None if k else apart)
+
+    order = [(i, j) for i in range(nh) for j in range(2)]
     for i, j in order:
-        produce(i, j, 0)
+        start_pair(i, j)
     for u in range(cuts[3]):
         beside(3, *near, u)
     for u in range(cuts[3]):
         for a in far:
             beside(3, *a, u)
     for i, j in order:
+        if i % 2 == 0:
+            finish_pair(i, j)
+    for i, j in order[: len(order) // 2]:
+        produce(i, j, 1)
+    for i, j in order:
+        if i % 2:
+            finish_pair(i, j)
+    for i, j in order[len(order) // 2 :]:
         produce(i, j, 1)
     columns = obuf.shape[2]
     for l in range(2):
         for i, j in order:
-            index = sp_of((zh + i) % nh, (zl + j) % 2, (y + l) % 2)
-
-            def keep(index=index):
-                rsbuf[index, g] = outbuf[index, pl.ds(pl.multiple_of(t * rows, rows), rows)]
-
-            receive(rsbuf.at[index, pl.ds(0, m - 1)], r_recv.at[index], own)
+            index = slice_of(i, j, l)
+            if l:
+                spot, count = g, m
+            elif i % 2:
+                spot, count = x, nx
+            else:
+                spot, count = zl, 2
+
+            def keep(index=index, spot=spot):
+                rsbuf[index, spot] = outbuf[index, pl.ds(pl.multiple_of(t * rows, rows), rows)]
+
+            receive(rsbuf.at[index, pl.ds(0, count - 1)], r_recv.at[index], own)
             pl.when(own)(keep)
-            receive(rsbuf.at[index], r_recv.at[index], apart)
+            receive(rsbuf.at[index, pl.ds(0, count)], r_recv.at[index], apart)
             total = rsbuf[index, 0].astype(F32)
-            for other in range(1, m):
+            for other in range(1, count):
                 total = total + rsbuf[index, other].astype(F32)
             span = pl.ds(pl.multiple_of(index * columns, columns), columns)
             out_ref[:, span] = total.astype(BF16)
@@ -674,12 +750,13 @@
             pltpu.VMEM((n + 1, deep_o, w_out_ret.shape[1]), BF16),
             pltpu.VMEM((n, tok, 2 * HEAD), BF16),
             pltpu.VMEM((n, tall, 2 * HEAD), BF16),
-            pltpu.VMEM((heads, HEAD, HEAD), F32),
+            pltpu.VMEM((heads, tok, tok), F32),
             pltpu.VMEM((heads * tok, 2 * HEAD), F32),
             pltpu.VMEM((heads * tok, 2 * HEAD), BF16),
             pltpu.VMEM((heads * tok, LANES), F32),
             pltpu.VMEM((n, tok, w_out_ret.shape[1]), BF16),
             pltpu.VMEM((n, m, rows, w_out_ret.shape[1]), BF16),
+            pltpu.VMEM((n, tok, w_out_ret.shape[1]), BF16),
             pltpu.VMEM((1, depth), F32),
             dma((9,)),
             dma((2,)),
@@ -698,6 +775,7 @@
             dma((2, nh, 2)),
             dma((2, n)),
             dma,
+            dma((n,)),
             dma((n,)),
         ],
         compiler_params=pltpu.CompilerParams(

time: 59.9 us -> 58.7 us (0.980)
  Pallas kernels: 58.1 us -> 56.8 us
    pallas_call x1, Pallas kernels: 58.1 us -> 56.8 us  [body(): pl.pallas_call(functools.partial(kernel, n, m, heads), out_shape=jax.Shap...]
where the time goes in v6:
time: 58.7 us; the launch traced here: 58.5 us
  Pallas kernels  56.8 us (97%)
  local copies, waits for them, and re-layouts  1.67 us (3%)
    pallas_call x1, Pallas kernels, body(): pl.pallas_call(functools.partial(kernel, n, m, heads), out_shape=jax.Shap...  56.8 us
    unnamed x1, local copies, waits for them, and re-layouts  1.67 us

profile of v6, /device:TPU:17, one launch (start us, length us, event | category | flops | bytes accessed | tf_op | source)
XLA Modules:
  0.0 58.5 jit_solution(9335572217703861940)
XLA Ops:
  0.0 56.8 %shard_map.127 = bf16[64,2048]{1,0:T(8,128)(2,1)} custom-call(bf16[64,2048]{1,0:T(8,128)(2,1)} %tok_hbm.1, f32[1,2048]{1,0:T(1,128)} %bitcast.14, bf16[192,256]{1,0:T(8,128)(2,1)} %bitcast.8, bf16[192,256]{1,0:T(8,128)(2,1)} %bitcast.9, bf16[192,256]{1,0:T(8,128)(2,1)} %bitcast.10, bf16[192,256]{1,0:T(8,128)(2,1)} %bitcast.11, bf16[64,256]{1,0:T(8,128)(2,1)} %bitcast.12, ...), custom_call_target="tpu_custom_call" | custom-call | tf_op jit(solution)/shard_map/pallas_call | solution.py:736
  56.8 1.7 %copy.15 = bf16[64,2048]{1,0:T(8,128)(2,1)} copy(bf16[64,2048]{1,0:T(8,128)(2,1)} %shard_map.127) | data formatting | bytes 524288

commit v7 on v6

--- a/solution.py
+++ b/solution.py
@@ -63,6 +63,7 @@
     outbuf,
     rsbuf,
     passed,
+    mixed,
     gain,
     load,
     small_send,
@@ -228,9 +229,9 @@
         for u in range(cuts[p]):
             scatter_one(p, 0, 1, u, own)
 
-    def scatter_near(p, u):
+    def scatter_near(p, u, also=True):
         for k in range(2):
-            scatter_one(p, 0, k, u, apart)
+            scatter_one(p, 0, k, u, apart & also)
 
     def scatter_far(p, u, condition=None):
         for i in range(1, nh):
@@ -519,8 +520,9 @@
 
     exchange_send(stbuf, 1)
     for u in range(1, cuts[3]):
+        scatter_near(3, u)
+    for u in range(1, cuts[3]):
         scatter_far(3, u, zh < nh - 1)
-        scatter_near(3, u)
     for a in far:
         entry(3, *a, 0)
     for u in range(cuts[2]):
@@ -542,6 +544,8 @@
         local.append(dot(weights, vals[h]))
         lifts.append((query.astype(F32) * jnp.exp(column)).astype(BF16))
     exchange_far(stbuf, 1, zl > c)
+    for u in range(1, cuts[3]):
+        entry(3, *near, u)
     exchange_far_part(kvbuf, 0)
 
     def attend_far(half):
@@ -552,11 +556,15 @@
     exchange_across(stbuf, 1)
     attend_far(0)
     attend_far(1)
+    for h in range(heads):
+        both = num[h * tok : (h + 1) * tok, :]
+        mixed[:, width + h * HEAD : width + (h + 1) * HEAD] = (
+            both[:, HEAD:] / both[:, :HEAD]
+        ).astype(BF16)
     exchange_far_across(stbuf, 1)
     for u in range(1, cuts[3]):
         for a in far:
             entry(3, *a, u)
-        entry(3, *near, u)
     exchange_part(stbuf, 1)
     exchange_far_part(stbuf, 1)
     states = [jnp.zeros((HEAD, HEAD), F32)] * heads
@@ -566,15 +574,13 @@
             total = marked[16 * h : 16 * h + 1] + marked[16 * h + 8 : 16 * h + 9]
             moved = jnp.exp(total) * states[h] + piece_of(j, h)
             states[h] = jnp.where(q > j, moved, states[h])
-    retained, attended = [], []
+    retained = []
     for h in range(heads):
         raw = local[h] + dot(lifts[h], states[h].astype(BF16))
         centre = jnp.mean(raw, axis=-1, keepdims=True)
         spread = jnp.mean(jnp.square(raw - centre), axis=-1, keepdims=True)
         retained.append(((raw - centre) * lax.rsqrt(spread + EPS)).astype(BF16))
-        both = num[h * tok : (h + 1) * tok, :]
-        attended.append((both[:, HEAD:] / both[:, :HEAD]).astype(BF16))
-    mixed = jnp.concatenate(retained + attended, axis=-1)
+    mixed[:, :width] = jnp.concatenate(retained, axis=-1)
     order = [(i, j) for i in range(nh) for j in range(2)]
 
     pair = 2 * rows
@@ -588,7 +594,7 @@
         receive(
             halves(3, 1), o_second.at[index], apart if i == 0 and j == 0 and l == 0 else None
         )
-        outbuf[index] = dot(mixed, obuf[index]).astype(BF16)
+        outbuf[index] = dot(mixed[...], obuf[index]).astype(BF16)
         return index
 
     def give(index, spot, x_, c_, condition):
@@ -652,19 +658,19 @@
         start_pair(i, j)
     for u in range(cuts[3]):
         beside(3, *near, u)
+    for i, j in order[:2]:
+        produce(i, j, 1)
     for u in range(cuts[3]):
         for a in far:
             beside(3, *a, u)
     for i, j in order:
         if i % 2 == 0:
             finish_pair(i, j)
-    for i, j in order[: len(order) // 2]:
+    for i, j in order[2:]:
         produce(i, j, 1)
     for i, j in order:
         if i % 2:
             finish_pair(i, j)
-    for i, j in order[len(order) // 2 :]:
-        produce(i, j, 1)
     columns = obuf.shape[2]
     for l in range(2):
         for i, j in order:
@@ -757,6 +763,7 @@
             pltpu.VMEM((n, tok, w_out_ret.shape[1]), BF16),
             pltpu.VMEM((n, m, rows, w_out_ret.shape[1]), BF16),
             pltpu.VMEM((n, tok, w_out_ret.shape[1]), BF16),
+            pltpu.VMEM((tok, 2 * heads * HEAD), BF16),
             pltpu.VMEM((1, depth), F32),
             dma((9,)),
             dma((2,)),

time: 58.7 us -> 57.6 us (0.981)
  Pallas kernels: 56.8 us -> 55.7 us
    pallas_call x1, Pallas kernels: 56.8 us -> 55.7 us  [body(): pl.pallas_call(functools.partial(kernel, n, m, heads), out_shape=jax.Shap...]
where the time goes in v7:
time: 57.6 us; the launch traced here: 57.4 us
  Pallas kernels  55.7 us (97%)
  local copies, waits for them, and re-layouts  1.67 us (3%)
    pallas_call x1, Pallas kernels, body(): pl.pallas_call(functools.partial(kernel, n, m, heads), out_shape=jax.Shap...  55.7 us
    unnamed x1, local copies, waits for them, and re-layouts  1.67 us

profile of v7, /device:TPU:17, one launch (start us, length us, event | category | flops | bytes accessed | tf_op | source)
XLA Modules:
  0.0 57.4 jit_solution(12428612165977473481)
XLA Ops:
  0.0 55.7 %shard_map.127 = bf16[64,2048]{1,0:T(8,128)(2,1)} custom-call(bf16[64,2048]{1,0:T(8,128)(2,1)} %tok_hbm.1, f32[1,2048]{1,0:T(1,128)} %bitcast.14, bf16[192,256]{1,0:T(8,128)(2,1)} %bitcast.8, bf16[192,256]{1,0:T(8,128)(2,1)} %bitcast.9, bf16[192,256]{1,0:T(8,128)(2,1)} %bitcast.10, bf16[192,256]{1,0:T(8,128)(2,1)} %bitcast.11, bf16[64,256]{1,0:T(8,128)(2,1)} %bitcast.12, ...), custom_call_target="tpu_custom_call" | custom-call | tf_op jit(solution)/shard_map/pallas_call | solution.py:742
  55.8 1.7 %copy.15 = bf16[64,2048]{1,0:T(8,128)(2,1)} copy(bf16[64,2048]{1,0:T(8,128)(2,1)} %shard_map.127) | data formatting | bytes 524288

commit v8 on v7

--- a/solution.py
+++ b/solution.py
@@ -545,7 +545,7 @@
         lifts.append((query.astype(F32) * jnp.exp(column)).astype(BF16))
     exchange_far(stbuf, 1, zl > c)
     for u in range(1, cuts[3]):
-        entry(3, *near, u)
+        entry(3, *near, u, zh == nh - 1)
     exchange_far_part(kvbuf, 0)
 
     def attend_far(half):
@@ -654,7 +654,10 @@
                 give(index, zl, x, (c + k) % 2, None if k else apart)
 
     order = [(i, j) for i in range(nh) for j in range(2)]
-    for i, j in order:
+    start_pair(*order[0])
+    for u in range(1, cuts[3]):
+        entry(3, *near, u, zh < nh - 1)
+    for i, j in order[2:] + order[1:2]:
         start_pair(i, j)
     for u in range(cuts[3]):
         beside(3, *near, u)

time: 57.6 us -> 57.3 us (level)
  no operation moved by 1% of the time
where the time goes in v8:
time: 57.3 us; the launch traced here: 57.1 us
  Pallas kernels  55.5 us (97%)
  local copies, waits for them, and re-layouts  1.67 us (3%)
    pallas_call x1, Pallas kernels, body(): pl.pallas_call(functools.partial(kernel, n, m, heads), out_shape=jax.Shap...  55.5 us
    unnamed x1, local copies, waits for them, and re-layouts  1.67 us

profile of v8, /device:TPU:17, one launch (start us, length us, event | category | flops | bytes accessed | tf_op | source)
XLA Modules:
  0.0 57.1 jit_solution(5101267433590473724)
XLA Ops:
  0.0 55.5 %shard_map.127 = bf16[64,2048]{1,0:T(8,128)(2,1)} custom-call(bf16[64,2048]{1,0:T(8,128)(2,1)} %tok_hbm.1, f32[1,2048]{1,0:T(1,128)} %bitcast.14, bf16[192,256]{1,0:T(8,128)(2,1)} %bitcast.8, bf16[192,256]{1,0:T(8,128)(2,1)} %bitcast.9, bf16[192,256]{1,0:T(8,128)(2,1)} %bitcast.10, bf16[192,256]{1,0:T(8,128)(2,1)} %bitcast.11, bf16[64,256]{1,0:T(8,128)(2,1)} %bitcast.12, ...), custom_call_target="tpu_custom_call" | custom-call | tf_op jit(solution)/shard_map/pallas_call | solution.py:745
  55.5 1.7 %copy.15 = bf16[64,2048]{1,0:T(8,128)(2,1)} copy(bf16[64,2048]{1,0:T(8,128)(2,1)} %shard_map.127) | data formatting | bytes 524288

commit v9 on v8

--- a/solution.py
+++ b/solution.py
@@ -17,7 +17,7 @@
 SPAN = 256
 KEY_SPAN = 256
 LANES = 128
-CUTS = (2, 2, 1, 3)
+CUTS = (2, 2, 1, 4)
 LOG2E = float(np.log2(np.e))
 TOKEN_CUT = 4
 HIGH = lax.Precision.HIGHEST

time: 57.3 us -> 57.5 us (level)
  no operation moved by 1% of the time
where the time goes in v9:
time: 57.5 us; the launch traced here: 57.2 us
  Pallas kernels  55.5 us (97%)
  local copies, waits for them, and re-layouts  1.67 us (3%)
    pallas_call x1, Pallas kernels, body(): pl.pallas_call(functools.partial(kernel, n, m, heads), out_shape=jax.Shap...  55.5 us
    unnamed x1, local copies, waits for them, and re-layouts  1.67 us

profile of v9, /device:TPU:17, one launch (start us, length us, event | category | flops | bytes accessed | tf_op | source)
XLA Modules:
  0.0 57.2 jit_solution(14675127583490800947)
XLA Ops:
  0.0 55.5 %shard_map.127 = bf16[64,2048]{1,0:T(8,128)(2,1)} custom-call(bf16[64,2048]{1,0:T(8,128)(2,1)} %tok_hbm.1, f32[1,2048]{1,0:T(1,128)} %bitcast.14, bf16[192,256]{1,0:T(8,128)(2,1)} %bitcast.8, bf16[192,256]{1,0:T(8,128)(2,1)} %bitcast.9, bf16[192,256]{1,0:T(8,128)(2,1)} %bitcast.10, bf16[192,256]{1,0:T(8,128)(2,1)} %bitcast.11, bf16[64,256]{1,0:T(8,128)(2,1)} %bitcast.12, ...), custom_call_target="tpu_custom_call" | custom-call | tf_op jit(solution)/shard_map/pallas_call | solution.py:745
  55.6 1.7 %copy.15 = bf16[64,2048]{1,0:T(8,128)(2,1)} copy(bf16[64,2048]{1,0:T(8,128)(2,1)} %shard_map.127) | data formatting | bytes 524288
